TPU v7x, 32 devices: a whole 2x2x4 slice. The times are simulated.
32 devices in a mesh: sp: 16 (over z, y, x), tp: 2 (over core).
Axes of the slice: x: 2, y: 2, z: 4, core: 2. Of those that a mesh axis runs over, the one named last changes fastest.
Arguments:
- queries: bfloat16 [3, 4096, 2048], P(None, 'sp', 'tp'), may hold values from -6 to 6
- keys: bfloat16 [3, 4096, 2048], P(None, 'sp', 'tp'), may hold values from -6 to 6
- values: bfloat16 [3, 4096, 2048], P(None, 'sp', 'tp'), may hold values from -6 to 6
- w_out: bfloat16 [2048, 2048], P(None, 'tp'), may hold values from -1 to 1
Outputs:
- mixed: bfloat16 [4096, 2048], P('sp', 'tp')
All inputs are finite; a program needn't handle non-finite values.
Results may differ from a plain program's by a relative error of at most 0.01.
Values may be sent and summed in bfloat16 or wider, within the bound.
A program may use at most 128 MiB of HBM per device.

v0:
```python
import functools

import jax
import jax.numpy as jnp
from jax import lax
from jax.experimental import pallas as pl
from jax.experimental.pallas import tpu as pltpu
from jax.sharding import PartitionSpec as P

HEAD = 128
KEYS = 128
STRIDES = (1, 4, 16)
ROPE_BASE = 10000.0
MASKED = -1e30
TEAM = 4

MESH = pl.DeviceIdType.MESH
F32 = jnp.float32
BF16 = jnp.bfloat16


def kernel(
    cfg,
    q_in, k_in, v_in, w_in, cos_ref, sin_ref,
    o_ref,
    raw, ready, w_buf, tables, perms, q_buf, kv0, kv1, kv2, acc, lse, bias, att, full, total_buf,
    in_sem, w_sem, deal_send, deal_recv, hop_send, hop_recv, ret_send, ret_recv, d2d_send, d2d_recv,
):
    tokens, n_sp, heads = cfg
    width = heads * HEAD
    mine = heads // TEAM
    part = mine * HEAD
    span = TEAM * tokens
    sp = lax.axis_index("sp")
    tp = lax.axis_index("tp")
    team = sp // TEAM
    me = lax.rem(sp, TEAM)
    has_next = sp + TEAM < n_sp
    has_prev = sp >= TEAM
    has_prev2 = sp >= 2 * TEAM

    inputs = (q_in, k_in, v_in)
    Q, K, V = 0, 1, 2
    order = [(V, 2), (K, 2), (V, 1), (K, 1), (V, 0), (K, 0), (Q, 2), (Q, 1), (Q, 0)]
    loads = {}
    for kind, g in order:
        copy = pltpu.make_async_copy(inputs[kind].at[g], raw.at[kind, g], in_sem.at[kind, g])
        copy.start()
        loads[kind, g] = copy
    w_loads = []
    for half in range(2):
        for head in range(mine):
            for s in range(TEAM):
                rows = pl.ds(half * width + s * part + head * HEAD, HEAD)
                copy = pltpu.make_async_copy(
                    w_in.at[rows],
                    w_buf.at[half, head, pl.ds(s * HEAD, HEAD)],
                    w_sem.at[half, head, s],
                )
                copy.start()
                w_loads.append(copy)

    barrier = pltpu.get_barrier_semaphore()
    for d in range(1, TEAM):
        peer = team * TEAM + lax.rem(me + d, TEAM)
        pl.semaphore_signal(barrier, inc=1, device_id={"sp": peer}, device_id_type=MESH)
    pl.semaphore_signal(barrier, inc=1, device_id={"tp": 1 - tp}, device_id_type=MESH)

    @pl.when(has_next)
    def _():
        pl.semaphore_signal(barrier, inc=1, device_id={"sp": sp + TEAM}, device_id_type=MESH)

    @pl.when(has_prev)
    def _():
        pl.semaphore_signal(barrier, inc=1, device_id={"sp": sp - TEAM}, device_id_type=MESH)

    row = lax.broadcasted_iota(jnp.int32, (tokens, tokens), 0)
    col = lax.broadcasted_iota(jnp.int32, (tokens, tokens), 1)

    def sorter(g):
        each = tokens // STRIDES[g]
        origin = lax.rem(row, each) * STRIDES[g] + row // each
        perms[g - 1] = jnp.where(origin == col, 1.0, 0.0).astype(BF16)

    def sort_tables(g):
        stride = STRIDES[g]
        each = tokens // stride
        for r in range(stride):
            tables[0, g, r * each : (r + 1) * each, :] = cos_ref[pl.ds(r, each, stride=stride), :]
            tables[1, g, r * each : (r + 1) * each, :] = sin_ref[pl.ds(r, each, stride=stride), :]

    def prepare(kind, g):
        loads[kind, g].wait()

        def step(h, carry):
            lanes = pl.ds(pl.multiple_of(h * HEAD, HEAD), HEAD)
            x = raw[kind, g, :, lanes]
            if g > 0:
                x = jnp.dot(perms[g - 1], x, preferred_element_type=F32)
            else:
                x = x.astype(F32)
            if kind != V:
                x = x * tables[0, g] + pltpu.roll(x, HEAD // 2, 1) * tables[1, g]
            if kind == Q:
                x = x * HEAD ** (-0.5)
            ready[kind, g, :, lanes] = x.astype(BF16)
            return carry

        lax.fori_loop(0, heads, step, 0, unroll=2)

    def slot(kind, g, s):
        if kind == Q:
            return q_buf.at[g, s]
        if g == 2:
            return kv2.at[kind - 1, 2 * TEAM + s]
        if g == 1:
            return kv1.at[kind - 1, 2 + s]
        return kv0.at[kind - 1, pl.ds(pl.multiple_of(KEYS + s * tokens, KEYS), tokens)]

    def cols(head):
        return slice(head * HEAD, (head + 1) * HEAD)

    def lanes_of(j):
        return pl.ds(pl.multiple_of(j * part, part), part)

    def deal(kind, g, d):
        peer = lax.rem(me + d, TEAM)
        return pltpu.make_async_remote_copy(
            src_ref=ready.at[kind, g, :, lanes_of(peer)],
            dst_ref=slot(kind, g, me),
            send_sem=deal_send.at[kind, g, d],
            recv_sem=deal_recv.at[kind, g, d],
            device_id={"sp": team * TEAM + peer},
            device_id_type=MESH,
        )

    def source(d):
        return lax.rem(me + TEAM - d, TEAM)

    def wait_deal(kind, g, d):
        here = slot(kind, g, source(d))
        pltpu.make_async_remote_copy(
            src_ref=here, dst_ref=here,
            send_sem=deal_send.at[kind, g, d], recv_sem=deal_recv.at[kind, g, d],
            device_id={"sp": team * TEAM + source(d)}, device_id_type=MESH,
        ).wait_recv()

    near = TEAM * (1 + mine)

    def hop(kind, index, src, dst):
        return pltpu.make_async_remote_copy(
            src_ref=src, dst_ref=dst,
            send_sem=hop_send.at[kind - 1, index], recv_sem=hop_recv.at[kind - 1, index],
            device_id={"sp": lax.rem(sp + TEAM, n_sp)}, device_id_type=MESH,
        )

    def first_hop(kind, s):
        return hop(kind, s, kv2.at[kind - 1, 2 * TEAM + s], kv2.at[kind - 1, TEAM + s])

    def second_hop(kind, s, head):
        return hop(
            kind, TEAM * (1 + head) + s,
            kv2.at[kind - 1, TEAM + s, :, cols(head)], kv2.at[kind - 1, s, :, cols(head)],
        )

    def near_hop(kind, i):
        return hop(kind, near + i, kv1.at[kind - 1, TEAM + i], kv1.at[kind - 1, i])

    def edge_hop(kind):
        return hop(
            kind, near + 2,
            kv0.at[kind - 1, pl.ds(span, KEYS)], kv0.at[kind - 1, pl.ds(0, KEYS)],
        )

    def forward(kind, g, s):
        if g == 2:
            pl.when(has_next)(lambda: first_hop(kind, s).start())
        elif g == 1:
            pl.when(has_next & (s >= TEAM - 2))(lambda: near_hop(kind, s - (TEAM - 2)).start())
        else:
            pl.when(has_next & (s == TEAM - 1))(lambda: edge_hop(kind).start())

    def relay(d, head):
        s = source(d)
        for kind in (V, K):
            if head == 0:

                @pl.when(has_prev)
                def _():
                    first_hop(kind, s).wait_recv()

            @pl.when(has_prev & has_next)
            def _():
                second_hop(kind, s, head).start()

    def place(kind, g):
        slot(kind, g, me)[...] = ready[kind, g, :, lanes_of(me)]

    def arrive(g, d):
        for kind in (V, K):
            wait_deal(kind, g, d)
            forward(kind, g, source(d))

    barrier_waited = False
    for n, (kind, g) in enumerate(order):
        if kind == V and g > 0:
            sorter(g)
        if kind == K:
            sort_tables(g)
        prepare(kind, g)
        place(kind, g)
        if not barrier_waited:
            count = TEAM + has_next.astype(jnp.int32) + has_prev.astype(jnp.int32)
            pl.semaphore_wait(barrier, count)
            barrier_waited = True
        for d in range(1, TEAM):
            deal(kind, g, d).start()
        if kind != Q:
            forward(kind, g, me)
        if n == 3:
            arrive(2, 1)
        if n == 5:
            arrive(2, 2)
    arrive(2, 3)
    relay(0, 0)
    relay(1, 0)
    for d in range(1, TEAM):
        arrive(1, d)
    relay(2, 0)
    relay(3, 0)
    for d in range(1, TEAM):
        arrive(0, d)
    for head in range(1, mine):
        for d in range(TEAM):
            relay(d, head)

    @pl.when(jnp.logical_not(has_prev))
    def _():
        for kind in range(2):
            kv0[kind, 0:KEYS, :] = jnp.zeros((KEYS, part), BF16)
            for s in range(2):
                kv1[kind, s] = jnp.zeros((tokens, part), BF16)
            for s in range(TEAM):
                kv2[kind, TEAM + s] = jnp.zeros((tokens, part), BF16)

    @pl.when(jnp.logical_not(has_prev2))
    def _():
        for kind in range(2):
            for s in range(TEAM):
                kv2[kind, s] = jnp.zeros((tokens, part), BF16)

    few = tokens // STRIDES[2]

    def fill(index, rows):
        a = lax.broadcasted_iota(jnp.int32, (rows, rows + KEYS), 0)
        b = lax.broadcasted_iota(jnp.int32, (rows, rows + KEYS), 1)
        allowed = (b >= jnp.maximum(a, KEYS - index)) & (b <= a + KEYS)
        return jnp.where(allowed, 0.0, MASKED)

    bias[0] = fill(team * span, KEYS)
    bias[1] = fill(KEYS, KEYS)
    bias[2, 0 : TEAM * few, 0 : TEAM * few + KEYS] = fill(team * TEAM * few, TEAM * few)

    def attend(g, tiles):
        scores = [
            lax.dot_general(t[1], t[2], (((1,), (1,)), ((), ())), preferred_element_type=F32)
            + t[4]
            for t in tiles
        ]
        best = [jnp.max(x, axis=1, keepdims=True) for x in scores]
        weights = [jnp.exp(x - m) for x, m in zip(scores, best)]
        outs = [
            jnp.dot(p.astype(BF16), t[3], preferred_element_type=F32)
            for p, t in zip(weights, tiles)
        ]
        total = [jnp.sum(p, axis=1, keepdims=True) for p in weights]
        for t, out, m, l in zip(tiles, outs, best, total):
            rows = out.shape[0]
            where = pl.ds(t[5], rows, stride=STRIDES[g]) if g else pl.ds(t[5], rows)
            acc[g, t[0], where, :] = out / l
            lse[g, t[0], where, :] = jnp.broadcast_to(m + jnp.log(l), (rows, HEAD))

    def far(head):
        @pl.when(has_prev2)
        def _():
            for d in range(TEAM):
                for kind in (V, K):
                    second_hop(kind, source(d), head).wait_recv()

        off = bias[2, 0 : TEAM * few, 0 : TEAM * few + KEYS]
        for first in range(0, STRIDES[2], 4):
            tiles = []
            for r in range(first, first + 4):
                rows = slice(r * few, (r + 1) * few)
                query = q_buf[2, :, rows, cols(head)].reshape(TEAM * few, HEAD)
                key = kv2[0, :, rows, cols(head)].reshape(3 * TEAM * few, HEAD)
                value = kv2[1, :, rows, cols(head)].reshape(3 * TEAM * few, HEAD)
                tiles.append((head, query, key, value, off, r))
            attend(2, tiles)

    for d in range(1, TEAM):
        wait_deal(Q, 2, d)
    far(0)

    for d in range(1, TEAM):
        wait_deal(Q, 1, d)

    @pl.when(has_prev)
    def _():
        for kind in (V, K):
            for i in range(2):
                near_hop(kind, i).wait_recv()

    each = tokens // STRIDES[1]
    pair = KEYS // each

    def step1(n, carry):
        r, i = n // (TEAM // pair), lax.rem(n, TEAM // pair)
        rows = pl.ds(pl.multiple_of(r * each, each), each)
        tiles = []
        for head in range(mine):
            query = q_buf[1, pl.ds(i * pair, pair), rows, cols(head)].reshape(KEYS, HEAD)
            key = kv1[0, pl.ds(i * pair, 2 * pair), rows, cols(head)].reshape(2 * KEYS, HEAD)
            value = kv1[1, pl.ds(i * pair, 2 * pair), rows, cols(head)].reshape(2 * KEYS, HEAD)
            tiles.append((head, query, key, value,
                          bias[jnp.minimum(i, 1)], r + STRIDES[1] * KEYS * i))
        attend(1, tiles)
        return carry

    lax.fori_loop(0, STRIDES[1] * (TEAM // pair), step1, 0, unroll=2)

    for d in range(1, TEAM):
        wait_deal(Q, 0, d)

    @pl.when(has_prev)
    def _():
        for kind in (V, K):
            edge_hop(kind).wait_recv()

    per = tokens // KEYS

    def step0(n, carry):
        inner = pl.ds(pl.multiple_of(lax.rem(n, per) * KEYS, KEYS), KEYS)
        rows = pl.ds(pl.multiple_of(n * KEYS, KEYS), 2 * KEYS)
        tiles = []
        for head in range(mine):
            query = q_buf[0, n // per, inner, cols(head)]
            tiles.append((head, query, kv0[0, rows, cols(head)], kv0[1, rows, cols(head)],
                          bias[jnp.minimum(n, 1)], pl.multiple_of(n * KEYS, KEYS)))
        attend(0, tiles)
        return carry

    lax.fori_loop(0, span // KEYS, step0, 0, unroll=2)

    def merge(j, head):
        rows = pl.ds(pl.multiple_of(j * tokens, tokens), tokens)
        logs = [lse[g, head, rows, :] for g in range(3)]
        peak = jnp.maximum(jnp.maximum(logs[0], logs[1]), logs[2])
        upper = jnp.zeros((tokens, HEAD), F32)
        lower = jnp.zeros((tokens, HEAD), F32)
        for g in range(3):
            scale = jnp.exp(logs[g] - peak)
            upper = upper + scale * acc[g, head, rows, :]
            lower = lower + scale
        att[head, j] = (upper / lower).astype(BF16)

    def place_of(s):
        return pl.ds(pl.multiple_of(s * HEAD, HEAD), HEAD)

    def home(d, head):
        peer = lax.rem(me + d, TEAM)
        return pltpu.make_async_remote_copy(
            src_ref=att.at[head, peer], dst_ref=full.at[tp, head, :, place_of(me)],
            send_sem=ret_send.at[d, head], recv_sem=ret_recv.at[d, head],
            device_id={"sp": team * TEAM + peer}, device_id_type=MESH,
        )

    def wait_home(d, head):
        here = full.at[tp, head, :, place_of(source(d))]
        pltpu.make_async_remote_copy(
            src_ref=here, dst_ref=here,
            send_sem=ret_send.at[d, head], recv_sem=ret_recv.at[d, head],
            device_id={"sp": team * TEAM + source(d)}, device_id_type=MESH,
        ).wait_recv()

    def twin(d, half, head):
        here = full.at[half, head, :, place_of(source(d))]
        return pltpu.make_async_remote_copy(
            src_ref=here, dst_ref=here,
            send_sem=d2d_send.at[d, head], recv_sem=d2d_recv.at[d, head],
            device_id={"tp": 1 - tp}, device_id_type=MESH,
        )

    for copy in w_loads:
        copy.wait()
    for head in range(mine):
        if head:
            far(head)
        for d in (2, 1, 3, 0):
            merge(lax.rem(me + d, TEAM), head)
            if d:
                home(d, head).start()
        full[tp, head, :, place_of(me)] = att[head, me]
        twin(0, tp, head).start()
    for head in range(mine):
        for d in (1, 3, 2):
            wait_home(d, head)
            twin(d, tp, head).start()
        product = jnp.dot(full[tp, head], w_buf[tp, head], preferred_element_type=F32)
        for d in range(TEAM):
            twin(d, 1 - tp, head).wait_recv()
        product = product + jnp.dot(
            full[1 - tp, head], w_buf[1 - tp, head], preferred_element_type=F32
        )
        if head == 0:
            total_buf[...] = product
        elif head < mine - 1:
            total_buf[...] += product
        else:
            o_ref[...] = (total_buf[...] + product).astype(BF16)

    for kind, g in order:
        for d in range(1, TEAM):
            deal(kind, g, d).wait_send()
    for head in range(mine):
        for d in range(1, TEAM):
            home(d, head).wait_send()
        for d in range(TEAM):
            twin(d, tp, head).wait_send()

    @pl.when(has_next)
    def _():
        for kind in (V, K):
            for s in range(TEAM):
                first_hop(kind, s).wait_send()
            for i in range(2):
                near_hop(kind, i).wait_send()
            edge_hop(kind).wait_send()

    @pl.when(has_prev & has_next)
    def _():
        for kind in (V, K):
            for s in range(TEAM):
                for head in range(mine):
                    second_hop(kind, s, head).wait_send()


def shards(n_sp, queries, keys, values, w_out):
    tokens, width = queries.shape[1:]
    heads = width // HEAD
    mine = heads // TEAM
    part = mine * HEAD
    span = TEAM * tokens
    start = lax.axis_index("sp") * tokens
    positions = (lax.iota(jnp.int32, tokens) + start).astype(F32)
    inverse = ROPE_BASE ** (-jnp.arange(0, HEAD, 2, dtype=F32) / HEAD)
    angles = positions[:, None] * inverse[None, :]
    cosine, sine = jnp.cos(angles), jnp.sin(angles)
    cosine = jnp.concatenate([cosine, cosine], axis=1)
    sine = jnp.concatenate([-sine, sine], axis=1)
    any_spec = pl.BlockSpec(memory_space=pl.ANY)
    vmem = pl.BlockSpec(memory_space=pltpu.VMEM)
    dma = pltpu.SemaphoreType.DMA
    return pl.pallas_call(
        functools.partial(kernel, (tokens, n_sp, heads)),
        out_shape=jax.ShapeDtypeStruct((tokens, w_out.shape[1]), BF16),
        in_specs=[any_spec] * 4 + [vmem] * 2,
        out_specs=vmem,
        scratch_shapes=[
            pltpu.VMEM((3, 3, tokens, width), BF16),
            pltpu.VMEM((3, 3, tokens, width), BF16),
            pltpu.VMEM((2, mine, TEAM * HEAD, w_out.shape[1]), BF16),
            pltpu.VMEM((2, 3, tokens, HEAD), F32),
            pltpu.VMEM((2, tokens, tokens), BF16),
            pltpu.VMEM((3, TEAM, tokens, part), BF16),
            pltpu.VMEM((2, KEYS + span, part), BF16),
            pltpu.VMEM((2, 2 + TEAM, tokens, part), BF16),
            pltpu.VMEM((2, 3 * TEAM, tokens, part), BF16),
            pltpu.VMEM((3, mine, span, HEAD), F32),
            pltpu.VMEM((3, mine, span, HEAD), F32),
            pltpu.VMEM((3, KEYS, 2 * KEYS), F32),
            pltpu.VMEM((mine, TEAM, tokens, HEAD), BF16),
            pltpu.VMEM((2, mine, tokens, TEAM * HEAD), BF16),
            pltpu.VMEM((tokens, w_out.shape[1]), F32),
            dma((3, 3)),
            dma((2, mine, TEAM)),
            dma((3, 3, TEAM)),
            dma((3, 3, TEAM)),
            dma((2, TEAM * (1 + mine) + 3)),
            dma((2, TEAM * (1 + mine) + 3)),
            dma((TEAM, mine)),
            dma((TEAM, mine)),
            dma((TEAM, mine)),
            dma((TEAM, mine)),
        ],
        compiler_params=pltpu.CompilerParams(
            collective_id=0, has_side_effects=True, vmem_limit_bytes=60 * 1024 * 1024
        ),
    )(queries, keys, values, w_out, cosine, sine)


def solution(mesh):
    return jax.shard_map(
        functools.partial(shards, mesh.shape["sp"]),
        mesh=mesh,
        in_specs=(P(None, "sp", "tp"), P(None, "sp", "tp"), P(None, "sp", "tp"), P(None, "tp")),
        out_specs=P("sp", "tp"),
        check_vma=False,
    )
```

profile of v0, /device:TPU:17, one launch (start us, length us, event | category | flops | bytes accessed | tf_op | source)
XLA Modules:
  0.0 79.0 jit_solution(17921909122780633788)
XLA Ops:
  0.0 0.5 fusion
  0.6 0.8 %pad_maximum_fusion = (f32[256,128]{1,0:T(8,128)}, f32[256,128]{1,0:T(8,128)}) fusion(f32[256,64]{1,0:T(8,128)S(1)} %get-tuple-element.7, f32[256,64]{1,0:T(8,128)S(1)} %get-tuple-element.6, f32[256,64]{1,0:T(8,128)S(1)} %get-tuple-element.5), kind=kLoop, calls=%fused_computation.2 | loop fusion | flops 65536 | bytes 458752 | tf_op jit(solution)/shard_map/concatenate | solution.py:459
  1.4 75.7 %shard_map.46 = bf16[256,1024]{1,0:T(8,128)(2,1)} custom-call(bf16[3,256,1024]{2,1,0:T(8,128)(2,1)} %q_in.1, bf16[3,256,1024]{2,1,0:T(8,128)(2,1)} %k_in.1, bf16[3,256,1024]{2,1,0:T(8,128)(2,1)} %v_in.1, bf16[2048,1024]{1,0:T(8,128)(2,1)} %w_in.1, f32[256,128]{1,0:T(8,128)} %get-tuple-element.8.cos_ref, f32[256,128]{1,0:T(8,128)} %get-tuple-element.9.sin_ref), custom_call_target="tpu_custom_call" | custom-call | tf_op jit(solution)/shard_map/pallas_call | solution.py:464
  77.1 1.9 %copy.6 = bf16[256,1024]{1,0:T(8,128)(2,1)} copy(bf16[256,1024]{1,0:T(8,128)(2,1)} %shard_map.46) | data formatting | bytes 1048576
  (2 shorter events, 0.0 us)
where the time goes:
time: 80.1 us; the launch traced here: 79 us
  Pallas kernels  75.7 us (95%)
  local copies, waits for them, and re-layouts  1.87 us (2%)
  other arithmetic  1.39 us (2%)
    pallas_call x1, Pallas kernels, shards(): pl.pallas_call(functools.partial(kernel, (tokens, n_sp, heads)), out_shap...  75.7 us
    unnamed x1, local copies, waits for them, and re-layouts  1.87 us

commit v1 on v0

v1 whole, which is shorter than its diff:
```python
import functools

import jax
import jax.numpy as jnp
import numpy as np
from jax import lax
from jax.experimental import pallas as pl
from jax.experimental.pallas import tpu as pltpu
from jax.sharding import PartitionSpec as P

HEAD = 128
KEYS = 128
STRIDES = (1, 4, 16)
ROPE_BASE = 10000.0
MASKED = -1e30
TEAM = 4

MESH = pl.DeviceIdType.MESH
F32 = jnp.float32
BF16 = jnp.bfloat16
Q, K, V = 0, 1, 2


def kernel(
    cfg,
    q_in, k_in, v_in, w_in, rows_in, base_in,
    o_ref,
    raw, ready, w_buf, rows_buf, base_buf, tables, perms,
    q_buf, q_next, kv0, kv1, kv2, acc, lse, acc1, lse1, bias,
    part_out, stat_out, part_in, stat_in, att, att_stat, back, back_stat, full, total_buf,
    in_sem, w_sem, t_sem, deal_send, deal_recv, first_send, first_recv, near_send, near_recv,
    turn_send, turn_recv, edge_send, edge_recv, part_send, part_recv, stat_send, stat_recv,
    ret_send, ret_recv, mark_send, mark_recv, d2d_send, d2d_recv,
):
    tokens, n_sp, heads = cfg
    width = heads * HEAD
    mine = heads // TEAM
    part = mine * HEAD
    span = TEAM * tokens
    few = tokens // STRIDES[2]
    lot = TEAM * few
    chunks = tokens // KEYS
    sp = lax.axis_index("sp")
    tp = lax.axis_index("tp")
    team = sp // TEAM
    me = lax.rem(sp, TEAM)
    has_next = sp + TEAM < n_sp
    has_prev = sp >= TEAM
    has_prev2 = sp >= 2 * TEAM
    middle = has_prev & has_next
    edge_next = sp + 1 < n_sp
    edge_prev = sp >= 1

    def partner(d):
        if d == 0:
            return me
        if d == 1:
            return me + 1 - 2 * lax.rem(me, 2)
        if d == 2:
            return lax.rem(me + 2, TEAM)
        return TEAM - 1 - me

    def cols(head):
        return slice(head * HEAD, (head + 1) * HEAD)

    def lanes_of(j):
        return pl.ds(pl.multiple_of(j * part, part), part)

    inputs = (q_in, k_in, v_in)
    loads = {}

    def load(kind, g):
        if (kind, g) == (V, 0):
            target = kv0.at[1, pl.ds(KEYS, tokens)]
        else:
            target = raw.at[kind, g]
        copy = pltpu.make_async_copy(inputs[kind].at[g], target, in_sem.at[kind, g])
        copy.start()
        loads[kind, g] = copy

    load(V, 2)
    rows_copy = pltpu.make_async_copy(rows_in, rows_buf, t_sem.at[0])
    rows_copy.start()
    base_copy = pltpu.make_async_copy(base_in, base_buf, t_sem.at[1])
    base_copy.start()
    for kind, g in ((K, 2), (Q, 2), (V, 1), (K, 1), (V, 0), (K, 0), (Q, 1), (Q, 0)):
        load(kind, g)
    w_loads = []
    for half in range(2):
        for head in range(mine):
            for s in range(TEAM):
                rows = pl.ds(half * width + s * part + head * HEAD, HEAD)
                copy = pltpu.make_async_copy(
                    w_in.at[rows],
                    w_buf.at[half, head, pl.ds(s * HEAD, HEAD)],
                    w_sem.at[half, head, s],
                )
                copy.start()
                w_loads.append(copy)

    barrier = pltpu.get_barrier_semaphore()

    def greet(where, when=None):
        def signal():
            pl.semaphore_signal(barrier, inc=1, device_id=where, device_id_type=MESH)

        if when is None:
            signal()
        else:
            pl.when(when)(signal)

    for d in range(1, TEAM):
        greet({"sp": team * TEAM + partner(d)})
    greet({"tp": 1 - tp})
    far_next = edge_next & (me == TEAM - 1)
    far_prev = edge_prev & (me == 0)
    greet({"sp": sp + TEAM}, has_next)
    greet({"sp": sp - TEAM}, has_prev)
    greet({"sp": sp + 1}, far_next)
    greet({"sp": sp - 1}, far_prev)

    row = lax.broadcasted_iota(jnp.int32, (tokens, tokens), 0)
    col = lax.broadcasted_iota(jnp.int32, (tokens, tokens), 1)

    def sorter(g):
        each = tokens // STRIDES[g]
        origin = lax.rem(row, each) * STRIDES[g] + row // each
        perms[g - 1] = jnp.where(origin == col, 1.0, 0.0).astype(BF16)

    def make_tables(g):
        c0, s0 = base_buf[sp, 0:1, :], base_buf[sp, 1:2, :]
        c, s = rows_buf[0, g], rows_buf[1, g]
        tables[0, g] = c0 * c - s0 * s
        tables[1, g] = s0 * c + c0 * s

    def turned(x, kind, g):
        x = x * tables[0, g] + pltpu.roll(x, HEAD // 2, 1) * tables[1, g]
        return x * HEAD ** (-0.5) if kind == Q else x

    def slot(kind, g, s):
        if kind == Q:
            return q_buf.at[g - 1, s]
        if g == 2:
            return kv2.at[kind - 1, TEAM + s]
        return kv1.at[kind - 1, 2 + s]

    def prepare(kind, g, d):
        j = partner(d)
        x = jnp.dot(perms[g - 1], raw[kind, g, :, lanes_of(j)], preferred_element_type=F32)
        for head in range(mine):
            y = x[:, cols(head)]
            if kind != V:
                y = turned(y, kind, g)
            if d == 0:
                slot(kind, g, me)[:, cols(head)] = y.astype(BF16)
            else:
                where = pl.ds(pl.multiple_of(j * part + head * HEAD, HEAD), HEAD)
                ready[kind, g - 1, :, where] = y.astype(BF16)

    def deal(kind, g, d):
        return pltpu.make_async_remote_copy(
            src_ref=ready.at[kind, g - 1, :, lanes_of(partner(d))],
            dst_ref=slot(kind, g, me),
            send_sem=deal_send.at[kind, g - 1, d],
            recv_sem=deal_recv.at[kind, g - 1, d],
            device_id={"sp": team * TEAM + partner(d)},
            device_id_type=MESH,
        )

    def wait_deal(kind, g, d):
        here = slot(kind, g, partner(d))
        pltpu.make_async_remote_copy(
            src_ref=here, dst_ref=here,
            send_sem=deal_send.at[kind, g - 1, d], recv_sem=deal_recv.at[kind, g - 1, d],
            device_id={"sp": team * TEAM + partner(d)}, device_id_type=MESH,
        ).wait_recv()

    def onward(src, dst, send, recv, to):
        return pltpu.make_async_remote_copy(
            src_ref=src, dst_ref=dst, send_sem=send, recv_sem=recv,
            device_id={"sp": lax.rem(to + n_sp, n_sp)}, device_id_type=MESH,
        )

    def first_hop(kind, s):
        return onward(
            kv2.at[kind - 1, TEAM + s], kv2.at[kind - 1, s],
            first_send.at[kind - 1, s], first_recv.at[kind - 1, s], sp + TEAM,
        )

    def near_hop(kind, i):
        return onward(
            kv1.at[kind - 1, TEAM + i], kv1.at[kind - 1, i],
            near_send.at[kind - 1, i], near_recv.at[kind - 1, i], sp + TEAM,
        )

    def turn_hop(s):
        return onward(q_buf.at[1, s], q_next.at[s], turn_send.at[s], turn_recv.at[s], sp - TEAM)

    def edge_hop(kind):
        return onward(
            kv0.at[kind - 1, pl.ds(tokens, KEYS)], kv0.at[kind - 1, pl.ds(0, KEYS)],
            edge_send.at[kind - 1], edge_recv.at[kind - 1], sp + 1,
        )

    def part_hop(head, j):
        rows = pl.ds(j * tokens, tokens)
        return onward(
            part_out.at[head, rows], part_in.at[head, rows],
            part_send.at[head, j], part_recv.at[head, j], sp + TEAM,
        )

    def stat_hop(head):
        return onward(
            stat_out.at[head], stat_in.at[head], stat_send.at[head], stat_recv.at[head], sp + TEAM,
        )

    def forward(kind, g, s):
        if kind == Q:
            if g == 2:
                pl.when(has_prev2)(lambda: turn_hop(s).start())
        elif g == 2:
            pl.when(has_next)(lambda: first_hop(kind, s).start())
        else:
            pl.when(has_next & (s >= TEAM - 2))(lambda: near_hop(kind, s - (TEAM - 2)).start())

    def arrive(kind, g, d):
        wait_deal(kind, g, d)
        forward(kind, g, partner(d))

    def send_all(kind, g, first=False):
        loads[kind, g].wait()
        for d in (3, 1, 2):
            prepare(kind, g, d)
            if first and d == 3:
                count = TEAM
                for extra in (has_next, has_prev, far_next, far_prev):
                    count = count + extra.astype(jnp.int32)
                pl.semaphore_wait(barrier, count)
            deal(kind, g, d).start()
        prepare(kind, g, 0)
        forward(kind, g, me)

    def own(kind):
        loads[kind, 0].wait()

        def step(h, carry):
            lanes = pl.ds(pl.multiple_of(h * HEAD, HEAD), HEAD)
            x = turned(raw[kind, 0, :, lanes].astype(F32), kind, 0).astype(BF16)
            if kind == K:
                kv0[0, KEYS:, lanes] = x
            else:
                ready[Q, 2, :, lanes] = x
            return carry

        lax.fori_loop(0, heads, step, 0, unroll=2)

    sorter(2)
    send_all(V, 2, first=True)
    rows_copy.wait()
    base_copy.wait()
    make_tables(2)
    send_all(K, 2)
    send_all(Q, 2)
    sorter(1)
    send_all(V, 1)
    for d in (1, 2, 3):
        arrive(V, 2, d)
    make_tables(1)
    send_all(K, 1)
    loads[V, 0].wait()
    pl.when(edge_next)(lambda: edge_hop(V).start())
    make_tables(0)
    own(K)
    pl.when(edge_next)(lambda: edge_hop(K).start())
    send_all(Q, 1)
    for d in (1, 2, 3):
        arrive(K, 2, d)
    own(Q)

    @pl.when(jnp.logical_not(edge_prev))
    def _():
        for kind in range(2):
            kv0[kind, 0:KEYS, :] = jnp.zeros((KEYS, width), BF16)

    @pl.when(jnp.logical_not(has_prev))
    def _():
        for kind in range(2):
            for s in range(2):
                kv1[kind, s] = jnp.zeros((tokens, part), BF16)
            for s in range(TEAM):
                kv2[kind, s] = jnp.zeros((tokens, part), BF16)

    @pl.when(jnp.logical_not(has_prev2))
    def _():
        for head in range(mine):
            part_in[head] = jnp.zeros((span, HEAD), BF16)
            stat_in[head] = jnp.full(stat_in.shape[1:], MASKED, F32)

    def band(index):
        a = lax.broadcasted_iota(jnp.int32, (KEYS, 2 * KEYS), 0)
        b = lax.broadcasted_iota(jnp.int32, (KEYS, 2 * KEYS), 1)
        allowed = (b >= jnp.maximum(a, KEYS - index)) & (b <= a + KEYS)
        return jnp.where(allowed, 0.0, MASKED)

    bias[0] = band(sp * tokens)
    bias[1] = band(KEYS)
    bias[2] = band(team * span)
    a = lax.broadcasted_iota(jnp.int32, (lot, 2 * lot), 0)
    b = lax.broadcasted_iota(jnp.int32, (lot, 2 * lot), 1)
    start = jnp.where(has_prev, 0, lot)
    bias[3, 0:lot, 0 : 2 * lot] = jnp.where((b <= a + lot) & (b >= start), 0.0, MASKED)
    bias[3, lot : 2 * lot, 0 : 2 * lot] = jnp.where(b >= a, 0.0, MASKED)

    def attend(tiles):
        scores = [
            lax.dot_general(t[0], t[1], (((1,), (1,)), ((), ())), preferred_element_type=F32)
            + t[3]
            for t in tiles
        ]
        best = [jnp.max(x, axis=1, keepdims=True) for x in scores]
        weights = [jnp.exp(x - m) for x, m in zip(scores, best)]
        outs = [
            jnp.dot(p.astype(BF16), t[2], preferred_element_type=F32)
            for p, t in zip(weights, tiles)
        ]
        total = [jnp.sum(p, axis=1, keepdims=True) for p in weights]
        for t, out, m, l in zip(tiles, outs, best, total):
            out_ref, log_ref, index, where = t[4]
            out_ref[(*index, where)] = out / l
            log_ref[(*index, where)] = jnp.broadcast_to(m + jnp.log(l), out.shape)

    def group1(n):
        def step(i, carry):
            tiles = []
            for u in range(mine):
                h = i * mine + u
                lanes = pl.ds(pl.multiple_of(h * HEAD, HEAD), HEAD)
                rows = slice(n * KEYS, (n + 2) * KEYS)
                tiles.append((
                    ready[Q, 2, n * KEYS : (n + 1) * KEYS, lanes],
                    kv0[0, rows, lanes], kv0[1, rows, lanes], bias[min(n, 1)],
                    (acc1, lse1, (h,), pl.ds(n * KEYS, KEYS)),
                ))
            attend(tiles)
            return carry

        lax.fori_loop(0, heads // mine, step, 0, unroll=2)

    def group2():
        each = tokens // STRIDES[1]
        pair = KEYS // each

        def step(n, carry):
            r, i = n // (TEAM // pair), lax.rem(n, TEAM // pair)
            rows = pl.ds(pl.multiple_of(r * each, each), each)
            tiles = []
            for head in range(mine):
                query = q_buf[0, pl.ds(i * pair, pair), rows, cols(head)].reshape(KEYS, HEAD)
                key = kv1[0, pl.ds(i * pair, 2 * pair), rows, cols(head)].reshape(2 * KEYS, HEAD)
                value = kv1[1, pl.ds(i * pair, 2 * pair), rows, cols(head)].reshape(2 * KEYS, HEAD)
                where = pl.ds(r + STRIDES[1] * KEYS * i, KEYS, stride=STRIDES[1])
                tiles.append((
                    query, key, value, bias[2 - jnp.minimum(i, 1)], (acc, lse, (0, head), where),
                ))
            attend(tiles)
            return carry

        lax.fori_loop(0, STRIDES[1] * (TEAM // pair), step, 0, unroll=2)

    def group3(head, queries, count, off, which):
        for first in range(0, STRIDES[2], 4):
            tiles = []
            for r in range(first, first + 4):
                rows = slice(r * few, (r + 1) * few)
                query = queries(rows).reshape(lot, HEAD)
                key = kv2[0, 0:count, rows, cols(head)].reshape(count * few, HEAD)
                value = kv2[1, 0:count, rows, cols(head)].reshape(count * few, HEAD)
                where = pl.ds(r, lot, stride=STRIDES[2])
                tiles.append((query, key, value, off, (acc, lse, (which, head), where)))
            attend(tiles)

    eye = (
        lax.broadcasted_iota(jnp.int32, (KEYS, KEYS), 0)
        == lax.broadcasted_iota(jnp.int32, (KEYS, KEYS), 1)
    )

    def to_row(x):
        return jnp.sum(jnp.where(eye, x, 0.0), axis=0, keepdims=True)

    def to_col(x):
        return jnp.sum(jnp.where(eye, x, 0.0), axis=1, keepdims=True)

    for d in (1, 2, 3):
        arrive(Q, 2, d)
    group1(1)
    for d in (1, 2, 3):
        arrive(V, 1, d)

    @pl.when(has_prev)
    def _():
        for s in range(TEAM):
            for kind in (V, K):
                first_hop(kind, s).wait_recv()

    @pl.when(middle)
    def _():
        for s in range(TEAM):
            turn_hop(s).wait_recv()
        off = bias[3, lot : 2 * lot, 0:lot]
        for head in range(mine):
            group3(head, lambda rows: q_next[:, rows, cols(head)], TEAM, off, 2)
            for j in range(TEAM):
                for c in range(j * chunks, (j + 1) * chunks):
                    rows = slice(c * KEYS, (c + 1) * KEYS)
                    part_out[head, rows] = acc[2, head, rows, :].astype(BF16)
                    stat_out[head, c : c + 1, :] = to_row(lse[2, head, rows, :])
                part_hop(head, j).start()
            stat_hop(head).start()

    for d in (1, 2, 3):
        arrive(K, 1, d)
    for head in range(mine):
        off = bias[3, 0:lot, 0 : 2 * lot]
        group3(head, lambda rows: q_buf[1, :, rows, cols(head)], 2 * TEAM, off, 1)

    @pl.when(edge_prev)
    def _():
        for kind in (V, K):
            edge_hop(kind).wait_recv()

    group1(0)
    for d in (1, 2, 3):
        wait_deal(Q, 1, d)

    @pl.when(has_prev)
    def _():
        for kind in (V, K):
            for i in range(2):
                near_hop(kind, i).wait_recv()

    group2()

    def merge(j, head, out_ref, log_ref):
        for c in range(chunks):
            rows = pl.ds(pl.multiple_of(j * tokens + c * KEYS, KEYS), KEYS)
            logs = [lse[g, head, rows, :] for g in range(2)]
            logs.append(to_col(stat_in[head, pl.ds(j * chunks + c, 1), :]))
            outs = [acc[g, head, rows, :] for g in range(2)]
            outs.append(part_in[head, rows, :].astype(F32))
            peak = jnp.maximum(jnp.maximum(logs[0], logs[1]), logs[2])
            scales = [jnp.exp(x - peak) for x in logs]
            lower = scales[0] + scales[1] + scales[2]
            upper = scales[0] * outs[0] + scales[1] * outs[1] + scales[2] * outs[2]
            out_ref[c * KEYS : (c + 1) * KEYS, :] = (upper / lower).astype(BF16)
            log_ref[c : c + 1, :] = to_row(peak + jnp.log(lower))

    def place_of(s):
        return pl.ds(pl.multiple_of(s * HEAD, HEAD), HEAD)

    def home(d, head):
        peer = partner(d)
        where = {"sp": team * TEAM + peer}
        return (
            pltpu.make_async_remote_copy(
                src_ref=att.at[head, peer], dst_ref=back.at[head, me],
                send_sem=ret_send.at[d, head], recv_sem=ret_recv.at[d, head],
                device_id=where, device_id_type=MESH,
            ),
            pltpu.make_async_remote_copy(
                src_ref=att_stat.at[head, peer], dst_ref=back_stat.at[head, me],
                send_sem=mark_send.at[d, head], recv_sem=mark_recv.at[d, head],
                device_id=where, device_id_type=MESH,
            ),
        )

    def wait_home(d, head):
        peer = partner(d)
        for ref, send, recv in (
            (back, ret_send, ret_recv), (back_stat, mark_send, mark_recv),
        ):
            here = ref.at[head, peer]
            pltpu.make_async_remote_copy(
                src_ref=here, dst_ref=here, send_sem=send.at[d, head], recv_sem=recv.at[d, head],
                device_id={"sp": team * TEAM + peer}, device_id_type=MESH,
            ).wait_recv()

    def finish(d, head):
        s = partner(d)
        h = s * mine + head
        for c in range(chunks):
            rows = slice(c * KEYS, (c + 1) * KEYS)
            log_a = lse1[h, rows, :]
            log_b = to_col(back_stat[head, s, c : c + 1, :])
            peak = jnp.maximum(log_a, log_b)
            scale_a, scale_b = jnp.exp(log_a - peak), jnp.exp(log_b - peak)
            upper = scale_a * acc1[h, rows, :] + scale_b * back[head, s, rows, :].astype(F32)
            full[tp, head, rows, place_of(s)] = (upper / (scale_a + scale_b)).astype(BF16)

    def twin(d, half, head):
        here = full.at[half, head, :, place_of(partner(d))]
        return pltpu.make_async_remote_copy(
            src_ref=here, dst_ref=here,
            send_sem=d2d_send.at[d, head], recv_sem=d2d_recv.at[d, head],
            device_id={"tp": 1 - tp}, device_id_type=MESH,
        )

    for copy in w_loads:
        copy.wait()
    for head in range(mine):

        @pl.when(has_prev2)
        def _():
            stat_hop(head).wait_recv()
            for j in range(TEAM):
                part_hop(head, j).wait_recv()

        for d in (3, 1, 2, 0):
            j = partner(d)
            if d:
                merge(j, head, att.at[head, j], att_stat.at[head, j])
                for copy in home(d, head):
                    copy.start()
            else:
                merge(j, head, back.at[head, j], back_stat.at[head, j])
        finish(0, head)
        twin(0, tp, head).start()
    for head in range(mine):
        for d in (1, 2, 3):
            wait_home(d, head)
            finish(d, head)
            twin(d, tp, head).start()
        product = jnp.dot(full[tp, head], w_buf[tp, head], preferred_element_type=F32)
        for d in range(TEAM):
            twin(d, 1 - tp, head).wait_recv()
        product = product + jnp.dot(
            full[1 - tp, head], w_buf[1 - tp, head], preferred_element_type=F32
        )
        if head == 0:
            total_buf[...] = product
        elif head < mine - 1:
            total_buf[...] += product
        else:
            o_ref[...] = (total_buf[...] + product).astype(BF16)

    for kind in range(3):
        for g in (1, 2):
            for d in range(1, TEAM):
                deal(kind, g, d).wait_send()
    for head in range(mine):
        for d in range(1, TEAM):
            for copy in home(d, head):
                copy.wait_send()
        for d in range(TEAM):
            twin(d, tp, head).wait_send()

    @pl.when(has_next)
    def _():
        for kind in (V, K):
            for s in range(TEAM):
                first_hop(kind, s).wait_send()
            for i in range(2):
                near_hop(kind, i).wait_send()

    @pl.when(edge_next)
    def _():
        for kind in (V, K):
            edge_hop(kind).wait_send()

    @pl.when(has_prev2)
    def _():
        for s in range(TEAM):
            turn_hop(s).wait_send()

    @pl.when(middle)
    def _():
        for head in range(mine):
            for j in range(TEAM):
                part_hop(head, j).wait_send()
            stat_hop(head).wait_send()


def angle_tables(tokens, n_sp):
    inverse = ROPE_BASE ** (-np.arange(0, HEAD, 2) / HEAD)

    def pair(positions):
        angles = positions[:, None] * inverse[None, :]
        cosine, sine = np.cos(angles), np.sin(angles)
        return (
            np.concatenate([cosine, cosine], axis=1),
            np.concatenate([-sine, sine], axis=1),
        )

    by_group = []
    for stride in STRIDES:
        order = np.arange(tokens).reshape(tokens // stride, stride).T.reshape(-1)
        by_group.append(pair(order.astype(np.float64)))
    rows = np.stack([np.stack([t[i] for t in by_group]) for i in range(2)])
    base = np.zeros((n_sp, 8, HEAD))
    base[:, 0], base[:, 1] = pair(np.arange(n_sp) * float(tokens))
    return rows.astype(np.float32), base.astype(np.float32)


def shards(n_sp, queries, keys, values, w_out):
    tokens, width = queries.shape[1:]
    heads = width // HEAD
    mine = heads // TEAM
    part = mine * HEAD
    span = TEAM * tokens
    rows, base = angle_tables(tokens, n_sp)
    any_spec = pl.BlockSpec(memory_space=pl.ANY)
    vmem = pl.BlockSpec(memory_space=pltpu.VMEM)
    dma = pltpu.SemaphoreType.DMA
    return pl.pallas_call(
        functools.partial(kernel, (tokens, n_sp, heads)),
        out_shape=jax.ShapeDtypeStruct((tokens, w_out.shape[1]), BF16),
        in_specs=[any_spec] * 6,
        out_specs=vmem,
        scratch_shapes=[
            pltpu.VMEM((3, 3, tokens, width), BF16),
            pltpu.VMEM((3, 3, tokens, width), BF16),
            pltpu.VMEM((2, mine, TEAM * HEAD, w_out.shape[1]), BF16),
            pltpu.VMEM(rows.shape, F32),
            pltpu.VMEM(base.shape, F32),
            pltpu.VMEM(rows.shape, F32),
            pltpu.VMEM((2, tokens, tokens), BF16),
            pltpu.VMEM((2, TEAM, tokens, part), BF16),
            pltpu.VMEM((TEAM, tokens, part), BF16),
            pltpu.VMEM((2, KEYS + tokens, width), BF16),
            pltpu.VMEM((2, 2 + TEAM, tokens, part), BF16),
            pltpu.VMEM((2, 2 * TEAM, tokens, part), BF16),
            pltpu.VMEM((3, mine, span, HEAD), F32),
            pltpu.VMEM((3, mine, span, HEAD), F32),
            pltpu.VMEM((heads, tokens, HEAD), F32),
            pltpu.VMEM((heads, tokens, HEAD), F32),
            pltpu.VMEM((4, KEYS, 2 * KEYS), F32),
            pltpu.VMEM((mine, span, HEAD), BF16),
            pltpu.VMEM((mine, span // KEYS, KEYS), F32),
            pltpu.VMEM((mine, span, HEAD), BF16),
            pltpu.VMEM((mine, span // KEYS, KEYS), F32),
            pltpu.VMEM((mine, TEAM, tokens, HEAD), BF16),
            pltpu.VMEM((mine, TEAM, 8, KEYS), F32),
            pltpu.VMEM((mine, TEAM, tokens, HEAD), BF16),
            pltpu.VMEM((mine, TEAM, 8, KEYS), F32),
            pltpu.VMEM((2, mine, tokens, TEAM * HEAD), BF16),
            pltpu.VMEM((tokens, w_out.shape[1]), F32),
            dma((3, 3)),
            dma((2, mine, TEAM)),
            dma((2,)),
            dma((3, 2, TEAM)),
            dma((3, 2, TEAM)),
            dma((2, TEAM)),
            dma((2, TEAM)),
            dma((2, 2)),
            dma((2, 2)),
            dma((TEAM,)),
            dma((TEAM,)),
            dma((2,)),
            dma((2,)),
            dma((mine, TEAM)),
            dma((mine, TEAM)),
            dma((mine,)),
            dma((mine,)),
            dma((TEAM, mine)),
            dma((TEAM, mine)),
            dma((TEAM, mine)),
            dma((TEAM, mine)),
            dma((TEAM, mine)),
            dma((TEAM, mine)),
        ],
        compiler_params=pltpu.CompilerParams(
            collective_id=0, has_side_effects=True, vmem_limit_bytes=60 * 1024 * 1024
        ),
    )(queries, keys, values, w_out, jnp.asarray(rows), jnp.asarray(base))


def solution(mesh):
    return jax.shard_map(
        functools.partial(shards, mesh.shape["sp"]),
        mesh=mesh,
        in_specs=(P(None, "sp", "tp"), P(None, "sp", "tp"), P(None, "sp", "tp"), P(None, "tp")),
        out_specs=P("sp", "tp"),
        check_vma=False,
    )
```

time: 80.1 us -> 77.3 us (0.965)
  other arithmetic: 1.39 us -> 0 us
    concatenate x1 -> x0, other arithmetic: 0.84 us -> none  [shards(): cosine = jnp.concatenate([cosine, cosine], axis=1)]
where the time goes in v1:
time: 77.3 us; the launch traced here: 76.9 us
  Pallas kernels  75.1 us (97%)
  local copies, waits for them, and re-layouts  1.87 us (2%)
    pallas_call x1, Pallas kernels, shards(): pl.pallas_call(functools.partial(kernel, (tokens, n_sp, heads)), out_shap...  75.1 us
    unnamed x1, local copies, waits for them, and re-layouts  1.87 us

profile of v1, /device:TPU:17, one launch (start us, length us, event | category | flops | bytes accessed | tf_op | source)
XLA Modules:
  0.0 76.9 jit_solution(12168900708108889935)
XLA Ops:
  0.0 75.1 %shard_map.64 = bf16[256,1024]{1,0:T(8,128)(2,1)} custom-call(bf16[3,256,1024]{2,1,0:T(8,128)(2,1)} %q_in.1, bf16[3,256,1024]{2,1,0:T(8,128)(2,1)} %k_in.1, bf16[3,256,1024]{2,1,0:T(8,128)(2,1)} %v_in.1, bf16[2048,1024]{1,0:T(8,128)(2,1)} %w_in.1, f32[2,3,256,128]{3,2,1,0:T(8,128)} %constant.4.clone.rows_in, f32[16,8,128]{2,1,0:T(8,128)} %constant.5.clone.base_in), custom_call_target="tpu_custom_call" | custom-call | tf_op jit(solution)/shard_map/pallas_call | solution.py:613
  75.1 1.9 %copy.8 = bf16[256,1024]{1,0:T(8,128)(2,1)} copy(bf16[256,1024]{1,0:T(8,128)(2,1)} %shard_map.64) | data formatting | bytes 1048576

commit v2 on v1

--- a/solution.py
+++ b/solution.py
@@ -23,13 +23,13 @@
 
 def kernel(
     cfg,
-    q_in, k_in, v_in, w_in, rows_in, base_in,
+    q_in, k_in, v_in, w_in, angles_in,
     o_ref,
-    raw, ready, w_buf, rows_buf, base_buf, tables, perms,
-    q_buf, q_next, kv0, kv1, kv2, acc, lse, acc1, lse1, bias,
+    raw, ready, w_buf, angles, tables, perms,
+    q_buf, q_next, kv0, kv1, kv2, relay, acc, lse, acc1, lse1, bias,
     part_out, stat_out, part_in, stat_in, att, att_stat, back, back_stat, full, total_buf,
     in_sem, w_sem, t_sem, deal_send, deal_recv, first_send, first_recv, near_send, near_recv,
-    turn_send, turn_recv, edge_send, edge_recv, part_send, part_recv, stat_send, stat_recv,
+    turn_send, turn_recv, edge_send, edge_recv, relay_send, relay_recv, part_send, part_recv, stat_send, stat_recv,
     ret_send, ret_recv, mark_send, mark_recv, d2d_send, d2d_recv,
 ):
     tokens, n_sp, heads = cfg
@@ -50,6 +50,8 @@
     middle = has_prev & has_next
     edge_next = sp + 1 < n_sp
     edge_prev = sp >= 1
+    relay_next = (me == TEAM - 2) & (sp + 2 < n_sp)
+    relay_prev = (me == 0) & (sp >= 2)
 
     def partner(d):
         if d == 0:
@@ -79,12 +81,183 @@
         loads[kind, g] = copy
 
     load(V, 2)
-    rows_copy = pltpu.make_async_copy(rows_in, rows_buf, t_sem.at[0])
-    rows_copy.start()
-    base_copy = pltpu.make_async_copy(base_in, base_buf, t_sem.at[1])
-    base_copy.start()
+    angles_copy = pltpu.make_async_copy(angles_in, angles, t_sem)
+    angles_copy.start()
     for kind, g in ((K, 2), (Q, 2), (V, 1), (K, 1), (V, 0), (K, 0), (Q, 1), (Q, 0)):
         load(kind, g)
+    barrier = pltpu.get_barrier_semaphore()
+
+    def greet(where, when=None):
+        def signal():
+            pl.semaphore_signal(barrier, inc=1, device_id=where, device_id_type=MESH)
+
+        if when is None:
+            signal()
+        else:
+            pl.when(when)(signal)
+
+    for d in range(1, TEAM):
+        greet({"sp": team * TEAM + partner(d)})
+    greet({"tp": 1 - tp})
+    far_next = edge_next & (me == TEAM - 1)
+    far_prev = edge_prev & (me == 0)
+    greet({"sp": sp + TEAM}, has_next)
+    greet({"sp": sp - TEAM}, has_prev)
+    greet({"sp": sp + 1}, far_next)
+    greet({"sp": sp - 1}, far_prev)
+    greet({"sp": sp + 2}, relay_next)
+    greet({"sp": sp - 2}, relay_prev)
+
+    row = lax.broadcasted_iota(jnp.int32, (tokens, tokens), 0)
+    col = lax.broadcasted_iota(jnp.int32, (tokens, tokens), 1)
+
+    def sorter(g):
+        each = tokens // STRIDES[g]
+        origin = lax.rem(row, each) * STRIDES[g] + row // each
+        perms[g - 1] = jnp.where(origin == col, 1.0, 0.0).astype(BF16)
+
+    def make_tables(g):
+        at = pl.multiple_of(6 * tokens + 8 * sp, 8)
+        base = angles[pl.ds(at, 8), :]
+        c0, s0 = base[0:1, :], base[1:2, :]
+        c = angles[g * tokens : (g + 1) * tokens, :]
+        s = angles[(3 + g) * tokens : (4 + g) * tokens, :]
+        tables[0, g] = c0 * c - s0 * s
+        tables[1, g] = s0 * c + c0 * s
+
+    def turned(x, kind, g):
+        x = x * tables[0, g] + pltpu.roll(x, HEAD // 2, 1) * tables[1, g]
+        return x * HEAD ** (-0.5) if kind == Q else x
+
+    def slot(kind, g, s):
+        if kind == Q:
+            return q_buf.at[g - 1, s]
+        if g == 2:
+            return kv2.at[kind - 1, TEAM + s]
+        return kv1.at[kind - 1, 2 + s]
+
+    def prepare(kind, g, d):
+        j = partner(d)
+        x = jnp.dot(perms[g - 1], raw[kind, g, :, lanes_of(j)], preferred_element_type=F32)
+        for head in range(mine):
+            y = x[:, cols(head)]
+            if kind != V:
+                y = turned(y, kind, g)
+            if d == 0:
+                slot(kind, g, me)[:, cols(head)] = y.astype(BF16)
+            else:
+                where = pl.ds(pl.multiple_of(j * part + head * HEAD, HEAD), HEAD)
+                ready[kind, g - 1, :, where] = y.astype(BF16)
+
+    def deal(kind, g, d):
+        return pltpu.make_async_remote_copy(
+            src_ref=ready.at[kind, g - 1, :, lanes_of(partner(d))],
+            dst_ref=slot(kind, g, me),
+            send_sem=deal_send.at[kind, g - 1, d],
+            recv_sem=deal_recv.at[kind, g - 1, d],
+            device_id={"sp": team * TEAM + partner(d)},
+            device_id_type=MESH,
+        )
+
+    def wait_deal(kind, g, d):
+        here = slot(kind, g, partner(d))
+        pltpu.make_async_remote_copy(
+            src_ref=here, dst_ref=here,
+            send_sem=deal_send.at[kind, g - 1, d], recv_sem=deal_recv.at[kind, g - 1, d],
+            device_id={"sp": team * TEAM + partner(d)}, device_id_type=MESH,
+        ).wait_recv()
+
+    def onward(src, dst, send, recv, to):
+        return pltpu.make_async_remote_copy(
+            src_ref=src, dst_ref=dst, send_sem=send, recv_sem=recv,
+            device_id={"sp": lax.rem(to + n_sp, n_sp)}, device_id_type=MESH,
+        )
+
+    def first_hop(kind, s):
+        return onward(
+            kv2.at[kind - 1, TEAM + s], kv2.at[kind - 1, s],
+            first_send.at[kind - 1, s], first_recv.at[kind - 1, s], sp + TEAM,
+        )
+
+    def near_hop(kind, i):
+        return onward(
+            kv1.at[kind - 1, TEAM + i], kv1.at[kind - 1, i],
+            near_send.at[kind - 1, i], near_recv.at[kind - 1, i], sp + TEAM,
+        )
+
+    def turn_hop(s):
+        return onward(q_buf.at[1, s], q_next.at[s], turn_send.at[s], turn_recv.at[s], sp - TEAM)
+
+    def edge_hop(kind):
+        return onward(
+            kv0.at[kind - 1, pl.ds(tokens, KEYS)], kv0.at[kind - 1, pl.ds(0, KEYS)],
+            edge_send.at[kind - 1], edge_recv.at[kind - 1], sp + 1,
+        )
+
+    def relay_in():
+        return onward(
+            kv0.at[1, pl.ds(tokens, KEYS)], relay, relay_send.at[0], relay_recv, sp - 1,
+        )
+
+    def relay_out():
+        return onward(
+            relay, kv0.at[1, pl.ds(0, KEYS)], relay_send.at[1], edge_recv.at[1], sp + 2,
+        )
+
+    def part_hop(head, j):
+        rows = pl.ds(j * tokens, tokens)
+        return onward(
+            part_out.at[head, rows], part_in.at[head, rows],
+            part_send.at[head, j], part_recv.at[head, j], sp + TEAM,
+        )
+
+    def stat_hop(head):
+        return onward(
+            stat_out.at[head], stat_in.at[head], stat_send.at[head], stat_recv.at[head], sp + TEAM,
+        )
+
+    def forward(kind, g, s):
+        if kind == Q:
+            if g == 2:
+                pl.when(has_prev2)(lambda: turn_hop(s).start())
+        elif g == 2:
+            pl.when(has_next)(lambda: first_hop(kind, s).start())
+        else:
+            pl.when(has_next & (s >= TEAM - 2))(lambda: near_hop(kind, s - (TEAM - 2)).start())
+
+    def arrive(kind, g, d):
+        wait_deal(kind, g, d)
+        forward(kind, g, partner(d))
+
+    def send_all(kind, g, first=False):
+        loads[kind, g].wait()
+        for d in (3, 1, 2):
+            prepare(kind, g, d)
+            if first and d == 3:
+                count = TEAM
+                for extra in (has_next, has_prev, far_next, far_prev, relay_next, relay_prev):
+                    count = count + extra.astype(jnp.int32)
+                pl.semaphore_wait(barrier, count)
+            deal(kind, g, d).start()
+        prepare(kind, g, 0)
+        forward(kind, g, me)
+
+    def own(kind):
+        loads[kind, 0].wait()
+
+        def step(h, carry):
+            lanes = pl.ds(pl.multiple_of(h * HEAD, HEAD), HEAD)
+            x = turned(raw[kind, 0, :, lanes].astype(F32), kind, 0).astype(BF16)
+            if kind == K:
+                kv0[0, KEYS:, lanes] = x
+            else:
+                ready[Q, 2, :, lanes] = x
+            return carry
+
+        lax.fori_loop(0, heads, step, 0, unroll=2)
+
+    sorter(2)
+    send_all(V, 2, first=True)
     w_loads = []
     for half in range(2):
         for head in range(mine):
@@ -97,167 +270,7 @@
                 )
                 copy.start()
                 w_loads.append(copy)
-
-    barrier = pltpu.get_barrier_semaphore()
-
-    def greet(where, when=None):
-        def signal():
-            pl.semaphore_signal(barrier, inc=1, device_id=where, device_id_type=MESH)
-
-        if when is None:
-            signal()
-        else:
-            pl.when(when)(signal)
-
-    for d in range(1, TEAM):
-        greet({"sp": team * TEAM + partner(d)})
-    greet({"tp": 1 - tp})
-    far_next = edge_next & (me == TEAM - 1)
-    far_prev = edge_prev & (me == 0)
-    greet({"sp": sp + TEAM}, has_next)
-    greet({"sp": sp - TEAM}, has_prev)
-    greet({"sp": sp + 1}, far_next)
-    greet({"sp": sp - 1}, far_prev)
-
-    row = lax.broadcasted_iota(jnp.int32, (tokens, tokens), 0)
-    col = lax.broadcasted_iota(jnp.int32, (tokens, tokens), 1)
-
-    def sorter(g):
-        each = tokens // STRIDES[g]
-        origin = lax.rem(row, each) * STRIDES[g] + row // each
-        perms[g - 1] = jnp.where(origin == col, 1.0, 0.0).astype(BF16)
-
-    def make_tables(g):
-        c0, s0 = base_buf[sp, 0:1, :], base_buf[sp, 1:2, :]
-        c, s = rows_buf[0, g], rows_buf[1, g]
-        tables[0, g] = c0 * c - s0 * s
-        tables[1, g] = s0 * c + c0 * s
-
-    def turned(x, kind, g):
-        x = x * tables[0, g] + pltpu.roll(x, HEAD // 2, 1) * tables[1, g]
-        return x * HEAD ** (-0.5) if kind == Q else x
-
-    def slot(kind, g, s):
-        if kind == Q:
-            return q_buf.at[g - 1, s]
-        if g == 2:
-            return kv2.at[kind - 1, TEAM + s]
-        return kv1.at[kind - 1, 2 + s]
-
-    def prepare(kind, g, d):
-        j = partner(d)
-        x = jnp.dot(perms[g - 1], raw[kind, g, :, lanes_of(j)], preferred_element_type=F32)
-        for head in range(mine):
-            y = x[:, cols(head)]
-            if kind != V:
-                y = turned(y, kind, g)
-            if d == 0:
-                slot(kind, g, me)[:, cols(head)] = y.astype(BF16)
-            else:
-                where = pl.ds(pl.multiple_of(j * part + head * HEAD, HEAD), HEAD)
-                ready[kind, g - 1, :, where] = y.astype(BF16)
-
-    def deal(kind, g, d):
-        return pltpu.make_async_remote_copy(
-            src_ref=ready.at[kind, g - 1, :, lanes_of(partner(d))],
-            dst_ref=slot(kind, g, me),
-            send_sem=deal_send.at[kind, g - 1, d],
-            recv_sem=deal_recv.at[kind, g - 1, d],
-            device_id={"sp": team * TEAM + partner(d)},
-            device_id_type=MESH,
-        )
-
-    def wait_deal(kind, g, d):
-        here = slot(kind, g, partner(d))
-        pltpu.make_async_remote_copy(
-            src_ref=here, dst_ref=here,
-            send_sem=deal_send.at[kind, g - 1, d], recv_sem=deal_recv.at[kind, g - 1, d],
-            device_id={"sp": team * TEAM + partner(d)}, device_id_type=MESH,
-        ).wait_recv()
-
-    def onward(src, dst, send, recv, to):
-        return pltpu.make_async_remote_copy(
-            src_ref=src, dst_ref=dst, send_sem=send, recv_sem=recv,
-            device_id={"sp": lax.rem(to + n_sp, n_sp)}, device_id_type=MESH,
-        )
-
-    def first_hop(kind, s):
-        return onward(
-            kv2.at[kind - 1, TEAM + s], kv2.at[kind - 1, s],
-            first_send.at[kind - 1, s], first_recv.at[kind - 1, s], sp + TEAM,
-        )
-
-    def near_hop(kind, i):
-        return onward(
-            kv1.at[kind - 1, TEAM + i], kv1.at[kind - 1, i],
-            near_send.at[kind - 1, i], near_recv.at[kind - 1, i], sp + TEAM,
-        )
-
-    def turn_hop(s):
-        return onward(q_buf.at[1, s], q_next.at[s], turn_send.at[s], turn_recv.at[s], sp - TEAM)
-
-    def edge_hop(kind):
-        return onward(
-            kv0.at[kind - 1, pl.ds(tokens, KEYS)], kv0.at[kind - 1, pl.ds(0, KEYS)],
-            edge_send.at[kind - 1], edge_recv.at[kind - 1], sp + 1,
-        )
-
-    def part_hop(head, j):
-        rows = pl.ds(j * tokens, tokens)
-        return onward(
-            part_out.at[head, rows], part_in.at[head, rows],
-            part_send.at[head, j], part_recv.at[head, j], sp + TEAM,
-        )
-
-    def stat_hop(head):
-        return onward(
-            stat_out.at[head], stat_in.at[head], stat_send.at[head], stat_recv.at[head], sp + TEAM,
-        )
-
-    def forward(kind, g, s):
-        if kind == Q:
-            if g == 2:
-                pl.when(has_prev2)(lambda: turn_hop(s).start())
-        elif g == 2:
-            pl.when(has_next)(lambda: first_hop(kind, s).start())
-        else:
-            pl.when(has_next & (s >= TEAM - 2))(lambda: near_hop(kind, s - (TEAM - 2)).start())
-
-    def arrive(kind, g, d):
-        wait_deal(kind, g, d)
-        forward(kind, g, partner(d))
-
-    def send_all(kind, g, first=False):
-        loads[kind, g].wait()
-        for d in (3, 1, 2):
-            prepare(kind, g, d)
-            if first and d == 3:
-                count = TEAM
-                for extra in (has_next, has_prev, far_next, far_prev):
-                    count = count + extra.astype(jnp.int32)
-                pl.semaphore_wait(barrier, count)
-            deal(kind, g, d).start()
-        prepare(kind, g, 0)
-        forward(kind, g, me)
-
-    def own(kind):
-        loads[kind, 0].wait()
-
-        def step(h, carry):
-            lanes = pl.ds(pl.multiple_of(h * HEAD, HEAD), HEAD)
-            x = turned(raw[kind, 0, :, lanes].astype(F32), kind, 0).astype(BF16)
-            if kind == K:
-                kv0[0, KEYS:, lanes] = x
-            else:
-                ready[Q, 2, :, lanes] = x
-            return carry
-
-        lax.fori_loop(0, heads, step, 0, unroll=2)
-
-    sorter(2)
-    send_all(V, 2, first=True)
-    rows_copy.wait()
-    base_copy.wait()
+    angles_copy.wait()
     make_tables(2)
     send_all(K, 2)
     send_all(Q, 2)
@@ -267,15 +280,23 @@
         arrive(V, 2, d)
     make_tables(1)
     send_all(K, 1)
-    loads[V, 0].wait()
-    pl.when(edge_next)(lambda: edge_hop(V).start())
+    send_all(Q, 1)
     make_tables(0)
     own(K)
-    pl.when(edge_next)(lambda: edge_hop(K).start())
-    send_all(Q, 1)
+    loads[V, 0].wait()
+
+    @pl.when(edge_next & (me < TEAM - 1))
+    def _():
+        for kind in (V, K):
+            edge_hop(kind).start()
+
+    @pl.when(far_next)
+    def _():
+        relay_in().start()
+
+    own(Q)
     for d in (1, 2, 3):
         arrive(K, 2, d)
-    own(Q)
 
     @pl.when(jnp.logical_not(edge_prev))
     def _():
@@ -390,9 +411,9 @@
     def to_col(x):
         return jnp.sum(jnp.where(eye, x, 0.0), axis=1, keepdims=True)
 
+    group1(1)
     for d in (1, 2, 3):
         arrive(Q, 2, d)
-    group1(1)
     for d in (1, 2, 3):
         arrive(V, 1, d)
 
@@ -402,12 +423,13 @@
             for kind in (V, K):
                 first_hop(kind, s).wait_recv()
 
-    @pl.when(middle)
-    def _():
-        for s in range(TEAM):
-            turn_hop(s).wait_recv()
-        off = bias[3, lot : 2 * lot, 0:lot]
-        for head in range(mine):
+    def pass_on(head):
+        @pl.when(middle)
+        def _():
+            if head == 0:
+                for s in range(TEAM):
+                    turn_hop(s).wait_recv()
+            off = bias[3, lot : 2 * lot, 0:lot]
             group3(head, lambda rows: q_next[:, rows, cols(head)], TEAM, off, 2)
             for j in range(TEAM):
                 for c in range(j * chunks, (j + 1) * chunks):
@@ -417,20 +439,26 @@
                 part_hop(head, j).start()
             stat_hop(head).start()
 
+    pass_on(0)
     for d in (1, 2, 3):
         arrive(K, 1, d)
+    for head in range(1, mine):
+        pass_on(head)
+
+    @pl.when(far_next)
+    def _():
+        edge_hop(K).start()
+
     for head in range(mine):
         off = bias[3, 0:lot, 0 : 2 * lot]
         group3(head, lambda rows: q_buf[1, :, rows, cols(head)], 2 * TEAM, off, 1)
-
-    @pl.when(edge_prev)
-    def _():
-        for kind in (V, K):
-            edge_hop(kind).wait_recv()
-
-    group1(0)
     for d in (1, 2, 3):
         wait_deal(Q, 1, d)
+
+    @pl.when(relay_next)
+    def _():
+        onward(relay, relay, relay_send.at[0], relay_recv, sp + 1).wait_recv()
+        relay_out().start()
 
     @pl.when(has_prev)
     def _():
@@ -522,6 +550,14 @@
                     copy.start()
             else:
                 merge(j, head, back.at[head, j], back_stat.at[head, j])
+
+    @pl.when(edge_prev)
+    def _():
+        for kind in (V, K):
+            edge_hop(kind).wait_recv()
+
+    group1(0)
+    for head in range(mine):
         finish(0, head)
         twin(0, tp, head).start()
     for head in range(mine):
@@ -561,10 +597,21 @@
             for i in range(2):
                 near_hop(kind, i).wait_send()
 
+    @pl.when(edge_next & (me < TEAM - 1))
+    def _():
+        edge_hop(V).wait_send()
+
     @pl.when(edge_next)
     def _():
-        for kind in (V, K):
-            edge_hop(kind).wait_send()
+        edge_hop(K).wait_send()
+
+    @pl.when(far_next)
+    def _():
+        relay_in().wait_send()
+
+    @pl.when(relay_next)
+    def _():
+        relay_out().wait_send()
 
     @pl.when(has_prev2)
     def _():
@@ -597,7 +644,7 @@
     rows = np.stack([np.stack([t[i] for t in by_group]) for i in range(2)])
     base = np.zeros((n_sp, 8, HEAD))
     base[:, 0], base[:, 1] = pair(np.arange(n_sp) * float(tokens))
-    return rows.astype(np.float32), base.astype(np.float32)
+    return np.concatenate([rows.reshape(-1, HEAD), base.reshape(-1, HEAD)]).astype(np.float32)
 
 
 def shards(n_sp, queries, keys, values, w_out):
@@ -606,28 +653,28 @@
     mine = heads // TEAM
     part = mine * HEAD
     span = TEAM * tokens
-    rows, base = angle_tables(tokens, n_sp)
+    angles = angle_tables(tokens, n_sp)
     any_spec = pl.BlockSpec(memory_space=pl.ANY)
     vmem = pl.BlockSpec(memory_space=pltpu.VMEM)
     dma = pltpu.SemaphoreType.DMA
     return pl.pallas_call(
         functools.partial(kernel, (tokens, n_sp, heads)),
         out_shape=jax.ShapeDtypeStruct((tokens, w_out.shape[1]), BF16),
-        in_specs=[any_spec] * 6,
+        in_specs=[any_spec] * 5,
         out_specs=vmem,
         scratch_shapes=[
             pltpu.VMEM((3, 3, tokens, width), BF16),
             pltpu.VMEM((3, 3, tokens, width), BF16),
             pltpu.VMEM((2, mine, TEAM * HEAD, w_out.shape[1]), BF16),
-            pltpu.VMEM(rows.shape, F32),
-            pltpu.VMEM(base.shape, F32),
-            pltpu.VMEM(rows.shape, F32),
+            pltpu.VMEM(angles.shape, F32),
+            pltpu.VMEM((2, 3, tokens, HEAD), F32),
             pltpu.VMEM((2, tokens, tokens), BF16),
             pltpu.VMEM((2, TEAM, tokens, part), BF16),
             pltpu.VMEM((TEAM, tokens, part), BF16),
             pltpu.VMEM((2, KEYS + tokens, width), BF16),
             pltpu.VMEM((2, 2 + TEAM, tokens, part), BF16),
             pltpu.VMEM((2, 2 * TEAM, tokens, part), BF16),
+            pltpu.VMEM((KEYS, width), BF16),
             pltpu.VMEM((3, mine, span, HEAD), F32),
             pltpu.VMEM((3, mine, span, HEAD), F32),
             pltpu.VMEM((heads, tokens, HEAD), F32),
@@ -645,7 +692,7 @@
             pltpu.VMEM((tokens, w_out.shape[1]), F32),
             dma((3, 3)),
             dma((2, mine, TEAM)),
-            dma((2,)),
+            dma,
             dma((3, 2, TEAM)),
             dma((3, 2, TEAM)),
             dma((2, TEAM)),
@@ -656,6 +703,8 @@
             dma((TEAM,)),
             dma((2,)),
             dma((2,)),
+            dma((2,)),
+            dma,
             dma((mine, TEAM)),
             dma((mine, TEAM)),
             dma((mine,)),
@@ -668,9 +717,9 @@
             dma((TEAM, mine)),
         ],
         compiler_params=pltpu.CompilerParams(
-            collective_id=0, has_side_effects=True, vmem_limit_bytes=60 * 1024 * 1024
+            collective_id=0, has_side_effects=True, vmem_limit_bytes=53 * 1024 * 1024
         ),
-    )(queries, keys, values, w_out, jnp.asarray(rows), jnp.asarray(base))
+    )(queries, keys, values, w_out, jnp.asarray(angles))
 
 
 def solution(mesh):

time: 77.3 us -> 70.7 us (0.915)
  Pallas kernels: 75.1 us -> 69.3 us
  local copies, waits for them, and re-layouts: 1.87 us -> 0.8 us
    pallas_call x1, Pallas kernels: 75.1 us -> 69.3 us  [shards(): pl.pallas_call(functools.partial(kernel, (tokens, n_sp, heads)), out_shap...]
    unnamed x1, local copies, waits for them, and re-layouts: 1.87 us -> 0.8 us
where the time goes in v2:
time: 70.7 us; the launch traced here: 70.1 us
  Pallas kernels  69.3 us (98%)
  local copies, waits for them, and re-layouts  0.8 us (1%)
    pallas_call x1, Pallas kernels, shards(): pl.pallas_call(functools.partial(kernel, (tokens, n_sp, heads)), out_shap...  69.3 us

profile of v2, /device:TPU:17, one launch (start us, length us, event | category | flops | bytes accessed | tf_op | source)
XLA Modules:
  0.0 70.1 jit_solution(14369175914629814090)
XLA Ops:
  0.0 69.3 %shard_map.55 = bf16[256,1024]{1,0:T(8,128)(2,1)S(1)} custom-call(bf16[3,256,1024]{2,1,0:T(8,128)(2,1)} %q_in.1, bf16[3,256,1024]{2,1,0:T(8,128)(2,1)} %k_in.1, bf16[3,256,1024]{2,1,0:T(8,128)(2,1)} %v_in.1, bf16[2048,1024]{1,0:T(8,128)(2,1)} %w_in.1, f32[1664,128]{1,0:T(8,128)} %constant.2.clone.angles_in), custom_call_target="tpu_custom_call" | custom-call | tf_op jit(solution)/shard_map/pallas_call | solution.py:660
  69.3 0.8 %copy.7 = bf16[256,1024]{1,0:T(8,128)(2,1)} copy(bf16[256,1024]{1,0:T(8,128)(2,1)S(1)} %shard_map.55) | data formatting | bytes 1048576

commit v3 on v2

v3 whole, which is shorter than its diff:
```python
import functools

import jax
import jax.numpy as jnp
import numpy as np
from jax import lax
from jax.experimental import pallas as pl
from jax.experimental.pallas import tpu as pltpu
from jax.sharding import PartitionSpec as P

HEAD = 128
KEYS = 128
STRIDES = (1, 4, 16)
ROPE_BASE = 10000.0
MASKED = -1e30
TEAM = 4

MESH = pl.DeviceIdType.MESH
F32 = jnp.float32
BF16 = jnp.bfloat16
Q, K, V = 0, 1, 2


def kernel(
    cfg,
    q_in, k_in, v_in, w_in, angles_in,
    o_ref,
    raw, ready, q_home, w_buf, angles, tables, perms,
    q_buf, q_next, q_near, kv0, kv1, kv2, relay, acc, lse, acc1, lse1, bias,
    part_out, stat_out, part_in, stat_in, near_out, mark_out, near_in, mark_in,
    att, att_stat, back, back_stat, full, total_buf,
    in_sem, w_sem, angles_sem, deal_send, deal_recv, pair_recv, first_send, first_recv,
    turn_send, turn_recv, low_send, low_recv, edge_send, edge_recv, relay_send, relay_recv,
    part_send, part_recv, stat_recv, near_send, near_recv, mark_recv,
    ret_send, ret_recv, tag_recv, d2d_send, d2d_recv,
):
    tokens, n_sp, heads = cfg
    width = heads * HEAD
    mine = heads // TEAM
    part = mine * HEAD
    span = TEAM * tokens
    few = tokens // STRIDES[2]
    lot = TEAM * few
    chunks = tokens // KEYS
    low = KEYS * STRIDES[1] // tokens
    sp = lax.axis_index("sp")
    tp = lax.axis_index("tp")
    team = sp // TEAM
    me = lax.rem(sp, TEAM)
    has_next = sp + TEAM < n_sp
    has_prev = sp >= TEAM
    has_prev2 = sp >= 2 * TEAM
    middle = has_prev & has_next
    edge_next = sp + 1 < n_sp
    edge_prev = sp >= 1
    relay_next = (me == 0) & has_next

    def partner(d):
        if d == 0:
            return me
        if d == 1:
            return me + 1 - 2 * lax.rem(me, 2)
        if d == 2:
            return lax.rem(me + 2, TEAM)
        return TEAM - 1 - me

    def cols(head):
        return slice(head * HEAD, (head + 1) * HEAD)

    def lanes_of(j):
        return pl.ds(pl.multiple_of(j * part, part), part)

    inputs = (q_in, k_in, v_in)
    loads = {}

    def load(kind, g):
        if (kind, g) == (V, 0):
            target = kv0.at[1, pl.ds(KEYS, tokens)]
        else:
            target = raw.at[kind, g]
        copy = pltpu.make_async_copy(inputs[kind].at[g], target, in_sem.at[kind, g])
        copy.start()
        loads[kind, g] = copy

    load(V, 2)
    angles_copy = pltpu.make_async_copy(angles_in, angles, angles_sem)
    angles_copy.start()
    for kind, g in ((K, 2), (Q, 2), (V, 1), (K, 1), (V, 0), (K, 0), (Q, 1), (Q, 0)):
        load(kind, g)
    barrier = pltpu.get_barrier_semaphore()

    def greet(where, when=None):
        def signal():
            pl.semaphore_signal(barrier, inc=1, device_id=where, device_id_type=MESH)

        if when is None:
            signal()
        else:
            pl.when(when)(signal)

    for d in range(1, TEAM):
        greet({"sp": team * TEAM + partner(d)})
    greet({"tp": 1 - tp})
    far_next = edge_next & (me == TEAM - 1)
    far_prev = edge_prev & (me == 0)
    greet({"sp": sp + TEAM}, has_next)
    greet({"sp": sp - TEAM}, has_prev)
    greet({"sp": sp + 1}, far_next)
    greet({"sp": sp - 1}, far_prev)

    row = lax.broadcasted_iota(jnp.int32, (tokens, tokens), 0)
    col = lax.broadcasted_iota(jnp.int32, (tokens, tokens), 1)

    def sorter(g):
        each = tokens // STRIDES[g]
        origin = lax.rem(row, each) * STRIDES[g] + row // each
        perms[g - 1] = jnp.where(origin == col, 1.0, 0.0).astype(BF16)

    def make_tables(g):
        at = pl.multiple_of(6 * tokens + 8 * sp, 8)
        base = angles[pl.ds(at, 8), :]
        c0, s0 = base[0:1, :], base[1:2, :]
        c = angles[g * tokens : (g + 1) * tokens, :]
        s = angles[(3 + g) * tokens : (4 + g) * tokens, :]
        tables[0, g] = c0 * c - s0 * s
        tables[1, g] = s0 * c + c0 * s

    def turned(x, kind, g):
        x = x * tables[0, g] + pltpu.roll(x, HEAD // 2, 1) * tables[1, g]
        return x * HEAD ** (-0.5) if kind == Q else x

    def slot(kind, g, head, s):
        if kind == Q:
            return q_buf.at[g - 1, head, s]
        if g == 2:
            return kv2.at[kind - 1, head, TEAM + s]
        return kv1.at[kind - 1, head, s]

    def prepare(kind, g, d):
        j = partner(d)
        x = jnp.dot(perms[g - 1], raw[kind, g, :, lanes_of(j)], preferred_element_type=F32)
        for head in range(mine):
            y = x[:, cols(head)]
            if kind != V:
                y = turned(y, kind, g)
            target = slot(kind, g, head, me) if d == 0 else ready.at[kind, g - 1, j, head]
            target[...] = y.astype(BF16)

    def recv_of(kind, g, head, d):
        if g == 1 and kind != Q:
            return pair_recv.at[head]
        return deal_recv.at[kind if g == 2 else 3, head, d - 1]

    def deal(kind, g, head, d):
        return pltpu.make_async_remote_copy(
            src_ref=ready.at[kind, g - 1, partner(d), head],
            dst_ref=slot(kind, g, head, me),
            send_sem=deal_send,
            recv_sem=recv_of(kind, g, head, d),
            device_id={"sp": team * TEAM + partner(d)},
            device_id_type=MESH,
        )

    def settle(ref, sem):
        pltpu.make_async_copy(ref, ref, sem).wait()

    def onward(src, dst, send, recv, to):
        return pltpu.make_async_remote_copy(
            src_ref=src, dst_ref=dst, send_sem=send, recv_sem=recv,
            device_id={"sp": lax.rem(to + n_sp, n_sp)}, device_id_type=MESH,
        )

    def first_hop(kind, head, s):
        return onward(
            kv2.at[kind - 1, head, TEAM + s], kv2.at[kind - 1, head, s],
            first_send, first_recv.at[head], sp + TEAM,
        )

    def turn_hop(head, s):
        return onward(
            q_buf.at[1, head, s], q_next.at[head, s], turn_send, turn_recv.at[head], sp - TEAM,
        )

    def low_hop(head, s):
        return onward(
            q_buf.at[0, head, s], q_near.at[head, s], low_send, low_recv.at[head], sp - TEAM,
        )

    def edge_hop(kind):
        return onward(
            kv0.at[kind - 1, pl.ds(tokens, KEYS)], kv0.at[kind - 1, pl.ds(0, KEYS)],
            edge_send, edge_recv, sp + 1,
        )

    def relay_in():
        return onward(
            kv0.at[1, pl.ds(tokens, KEYS)], relay, edge_send, relay_recv, sp - (TEAM - 1),
        )

    def relay_out():
        return onward(relay, kv0.at[1, pl.ds(0, KEYS)], relay_send, edge_recv, sp + TEAM)

    def part_hop(head, j):
        rows = pl.ds(j * tokens, tokens)
        return onward(
            part_out.at[head, rows], part_in.at[head, rows],
            part_send.at[0], part_recv.at[head], sp + TEAM,
        )

    def stat_hop(head):
        return onward(
            stat_out.at[head], stat_in.at[head], part_send.at[1], stat_recv.at[head], sp + TEAM,
        )

    def near_hop(head):
        return onward(
            near_out.at[head], near_in.at[head, pl.ds(0, near_out.shape[1])],
            near_send.at[0], near_recv.at[head], sp + TEAM,
        )

    def mark_hop(head):
        return onward(
            mark_out.at[head], mark_in.at[head], near_send.at[1], mark_recv.at[head], sp + TEAM,
        )

    def forward(kind, g, head, s):
        if g == 2 and kind == Q:
            pl.when(has_prev2)(lambda: turn_hop(head, s).start())
        elif g == 2:
            pl.when(has_next)(lambda: first_hop(kind, head, s).start())
        elif kind == Q:
            pl.when(has_prev & (s < low))(lambda: low_hop(head, s).start())

    def arrive(kind, g, head):
        for d in (1, 2, 3):
            s = partner(d)
            settle(slot(kind, g, head, s), recv_of(kind, g, head, d))
            forward(kind, g, head, s)

    def send_first(kind, g, first=False):
        loads[kind, g].wait()
        for d in (3, 1, 2, 0):
            prepare(kind, g, d)
            if first and d == 3:
                count = TEAM
                for extra in (has_next, has_prev, far_next, far_prev):
                    count = count + extra.astype(jnp.int32)
                pl.semaphore_wait(barrier, count)
            if d:
                deal(kind, g, 0, d).start()
            else:
                forward(kind, g, 0, me)

    def send_rest(kinds, g):
        for head in range(1, mine):
            for kind in kinds:
                for d in (3, 1, 2):
                    deal(kind, g, head, d).start()
                forward(kind, g, head, me)

    def own(kind):
        loads[kind, 0].wait()

        def step(h, carry):
            lanes = pl.ds(pl.multiple_of(h * HEAD, HEAD), HEAD)
            x = turned(raw[kind, 0, :, lanes].astype(F32), kind, 0).astype(BF16)
            if kind == K:
                kv0[0, KEYS:, lanes] = x
            else:
                q_home[:, lanes] = x
            return carry

        lax.fori_loop(0, heads, step, 0, unroll=2)

    sorter(2)
    send_first(V, 2, first=True)
    for half in range(2):
        for head in range(mine):
            for s in range(TEAM):
                rows = pl.ds(half * width + s * part + head * HEAD, HEAD)
                copy = pltpu.make_async_copy(
                    w_in.at[rows],
                    w_buf.at[half, head, pl.ds(s * HEAD, HEAD)],
                    w_sem,
                )
                copy.start()
    angles_copy.wait()
    make_tables(2)
    send_first(K, 2)
    send_first(Q, 2)
    send_rest((V, K, Q), 2)
    sorter(1)
    send_first(V, 1)
    make_tables(1)
    arrive(V, 2, 0)
    send_first(Q, 1)
    send_first(K, 1)
    send_rest((V, Q, K), 1)
    arrive(K, 2, 0)
    make_tables(0)
    own(K)
    loads[V, 0].wait()

    @pl.when(edge_next & (me < TEAM - 1))
    def _():
        for kind in (V, K):
            edge_hop(kind).start()

    @pl.when(far_next)
    def _():
        relay_in().start()

    own(Q)

    @pl.when(jnp.logical_not(edge_prev))
    def _():
        for kind in range(2):
            kv0[kind, 0:KEYS, :] = jnp.zeros((KEYS, width), BF16)

    @pl.when(jnp.logical_not(has_prev))
    def _():
        for kind in range(2):
            for s in range(TEAM):
                for head in range(mine):
                    kv2[kind, head, s] = jnp.zeros((tokens, HEAD), BF16)
        for head in range(mine):
            near_in[head] = jnp.zeros((span, HEAD), BF16)
            mark_in[head] = jnp.full(mark_in.shape[1:], MASKED, F32)

    @pl.when(jnp.logical_not(has_prev2))
    def _():
        for head in range(mine):
            part_in[head] = jnp.zeros((span, HEAD), BF16)
            stat_in[head] = jnp.full(stat_in.shape[1:], MASKED, F32)

    @pl.when(has_prev)
    def _():
        for head in range(mine):
            near_in[head, low * tokens :] = jnp.zeros((span - low * tokens, HEAD), BF16)

    for head in range(mine):
        mark_out[head] = jnp.full(mark_out.shape[1:], MASKED, F32)

    def band(index):
        a = lax.broadcasted_iota(jnp.int32, (KEYS, 2 * KEYS), 0)
        b = lax.broadcasted_iota(jnp.int32, (KEYS, 2 * KEYS), 1)
        allowed = (b >= jnp.maximum(a, KEYS - index)) & (b <= a + KEYS)
        return jnp.where(allowed, 0.0, MASKED)

    bias[0] = band(sp * tokens)
    bias[1] = band(KEYS)
    a = lax.broadcasted_iota(jnp.int32, (lot, 2 * lot), 0)
    b = lax.broadcasted_iota(jnp.int32, (lot, 2 * lot), 1)
    start = jnp.where(has_prev, 0, lot)
    bias[2, 0:lot, 0 : 2 * lot] = jnp.where((b <= a + lot) & (b >= start), 0.0, MASKED)
    bias[2, lot : 2 * lot, 0 : 2 * lot] = jnp.where(b >= a, 0.0, MASKED)

    def attend(tiles):
        scores = [
            lax.dot_general(t[0], t[1], (((1,), (1,)), ((), ())), preferred_element_type=F32)
            + t[3]
            for t in tiles
        ]
        best = [jnp.max(x, axis=1, keepdims=True) for x in scores]
        weights = [jnp.exp(x - m) for x, m in zip(scores, best)]
        outs = [
            jnp.dot(p.astype(BF16), t[2], preferred_element_type=F32)
            for p, t in zip(weights, tiles)
        ]
        total = [jnp.sum(p, axis=1, keepdims=True) for p in weights]
        for t, out, m, l in zip(tiles, outs, best, total):
            out_ref, log_ref, index, where = t[4]
            out_ref[(*index, where)] = out / l
            log_ref[(*index, where)] = jnp.broadcast_to(m + jnp.log(l), out.shape)

    def group1(n):
        def step(i, carry):
            tiles = []
            for u in range(mine):
                h = i * mine + u
                lanes = pl.ds(pl.multiple_of(h * HEAD, HEAD), HEAD)
                rows = slice(n * KEYS, (n + 2) * KEYS)
                tiles.append((
                    q_home[n * KEYS : (n + 1) * KEYS, lanes],
                    kv0[0, rows, lanes], kv0[1, rows, lanes], bias[min(n, 1)],
                    (acc1, lse1, (h,), pl.ds(n * KEYS, KEYS)),
                ))
            attend(tiles)
            return carry

        lax.fori_loop(0, heads // mine, step, 0, unroll=2)

    each = tokens // STRIDES[1]
    pair = KEYS // each

    def band2(source, first, count, r):
        rows = slice(r * each, (r + 1) * each)
        return source[first : first + count, rows, :].reshape(count * each, HEAD)

    def group2():
        for i in range(TEAM // pair):
            first = max(i - 1, 0) * pair
            count = (i + 1) * pair - first
            for r in range(STRIDES[1]):
                where = pl.ds(r + STRIDES[1] * KEYS * i, KEYS, stride=STRIDES[1])
                tiles = []
                for head in range(mine):
                    tiles.append((
                        band2(q_buf.at[0, head], i * pair, pair, r),
                        band2(kv1.at[0, head], first, count, r),
                        band2(kv1.at[1, head], first, count, r),
                        bias[1, :, 2 * KEYS - count * each :],
                        (acc, lse, (0, head), where),
                    ))
                attend(tiles)

    def group2_next(head):
        tiles = []
        for r in range(STRIDES[1]):
            tiles.append((
                band2(q_near.at[head], 0, pair, r),
                band2(kv1.at[0, head], TEAM - pair, pair, r),
                band2(kv1.at[1, head], TEAM - pair, pair, r),
                bias[1, :, 0:KEYS],
                (acc, lse, (3, head), pl.ds(r, KEYS, stride=STRIDES[1])),
            ))
        attend(tiles)

    def group3(head, queries, count, off, which):
        for first in range(0, STRIDES[2], 4):
            tiles = []
            for r in range(first, first + 4):
                rows = slice(r * few, (r + 1) * few)
                query = queries[:, rows, :].reshape(lot, HEAD)
                key = kv2[0, head, 0:count, rows, :].reshape(count * few, HEAD)
                value = kv2[1, head, 0:count, rows, :].reshape(count * few, HEAD)
                where = pl.ds(r, lot, stride=STRIDES[2])
                tiles.append((query, key, value, off, (acc, lse, (which, head), where)))
            attend(tiles)

    eye = (
        lax.broadcasted_iota(jnp.int32, (KEYS, KEYS), 0)
        == lax.broadcasted_iota(jnp.int32, (KEYS, KEYS), 1)
    )

    def to_row(x):
        return jnp.sum(jnp.where(eye, x, 0.0), axis=0, keepdims=True)

    def to_col(x):
        return jnp.sum(jnp.where(eye, x, 0.0), axis=1, keepdims=True)

    def store_part(slot_at, head, c, out_ref, log_ref):
        rows = slice(c * KEYS, (c + 1) * KEYS)
        out_ref[head, rows] = acc[slot_at, head, rows, :].astype(BF16)
        log_ref[head, c : c + 1, :] = to_row(lse[slot_at, head, rows, :])

    def first_done(head):
        @pl.when(has_prev)
        def _():
            settle(kv2.at[:, head, pl.ds(0, TEAM)], first_recv.at[head])

    def pass_on(head):
        @pl.when(middle)
        def _():
            settle(q_next.at[head], turn_recv.at[head])
            group3(head, q_next.at[head], TEAM, bias[2, lot : 2 * lot, 0:lot], 2)

    def pass_send(head):
        @pl.when(middle)
        def _():
            for j in range(TEAM):
                for c in range(j * chunks, (j + 1) * chunks):
                    store_part(2, head, c, part_out, stat_out)
                part_hop(head, j).start()
            stat_hop(head).start()

    def here(head):
        group3(head, q_buf.at[1, head], 2 * TEAM, bias[2, 0:lot, 0 : 2 * lot], 1)

    def low_pass(head):
        settle(kv1.at[:, head, pl.ds(0, TEAM - 1)], pair_recv.at[head])

        @pl.when(has_next)
        def _():
            settle(q_near.at[head], low_recv.at[head])
            group2_next(head)
            for c in range(low * chunks):
                store_part(3, head, c, near_out, mark_out)
            near_hop(head).start()
            mark_hop(head).start()

    arrive(Q, 2, 0)
    group1(1)
    arrive(V, 2, 1)
    first_done(0)
    pass_on(0)
    arrive(K, 2, 1)
    pass_send(0)
    here(0)
    arrive(Q, 2, 1)
    first_done(1)
    arrive(Q, 1, 0)
    pass_on(1)
    pass_send(1)
    here(1)
    low_pass(0)
    arrive(Q, 1, 1)
    low_pass(1)

    group2()

    def merge(j, head, out_ref, log_ref):
        for c in range(chunks):
            rows = pl.ds(pl.multiple_of(j * tokens + c * KEYS, KEYS), KEYS)
            logs = [lse[g, head, rows, :] for g in range(2)]
            logs.append(to_col(stat_in[head, pl.ds(j * chunks + c, 1), :]))
            logs.append(to_col(mark_in[head, pl.ds(j * chunks + c, 1), :]))
            outs = [acc[g, head, rows, :] for g in range(2)]
            outs.append(part_in[head, rows, :].astype(F32))
            outs.append(near_in[head, rows, :].astype(F32))
            peak = jnp.maximum(jnp.maximum(logs[0], logs[1]), jnp.maximum(logs[2], logs[3]))
            scales = [jnp.exp(x - peak) for x in logs]
            lower = sum(scales)
            upper = sum(x * y for x, y in zip(scales, outs))
            out_ref[c * KEYS : (c + 1) * KEYS, :] = (upper / lower).astype(BF16)
            log_ref[c : c + 1, :] = to_row(peak + jnp.log(lower))

    def place_of(s):
        return pl.ds(pl.multiple_of(s * HEAD, HEAD), HEAD)

    def home(d, head):
        peer = partner(d)
        where = {"sp": team * TEAM + peer}
        return (
            pltpu.make_async_remote_copy(
                src_ref=att.at[head, peer], dst_ref=back.at[head, me],
                send_sem=ret_send.at[0], recv_sem=ret_recv.at[d - 1, head],
                device_id=where, device_id_type=MESH,
            ),
            pltpu.make_async_remote_copy(
                src_ref=att_stat.at[head, peer], dst_ref=back_stat.at[head, me],
                send_sem=ret_send.at[1], recv_sem=tag_recv.at[d - 1, head],
                device_id=where, device_id_type=MESH,
            ),
        )

    def wait_home(d, head):
        settle(back.at[head, partner(d)], ret_recv.at[d - 1, head])
        settle(back_stat.at[head, partner(d)], tag_recv.at[d - 1, head])

    def finish(d, head):
        s = partner(d)
        h = s * mine + head
        for c in range(chunks):
            rows = slice(c * KEYS, (c + 1) * KEYS)
            log_a = lse1[h, rows, :]
            log_b = to_col(back_stat[head, s, c : c + 1, :])
            peak = jnp.maximum(log_a, log_b)
            scale_a, scale_b = jnp.exp(log_a - peak), jnp.exp(log_b - peak)
            upper = scale_a * acc1[h, rows, :] + scale_b * back[head, s, rows, :].astype(F32)
            full[tp, head, rows, place_of(s)] = (upper / (scale_a + scale_b)).astype(BF16)

    def twin(d, half, head):
        here = full.at[half, head, :, place_of(partner(d))]
        return pltpu.make_async_remote_copy(
            src_ref=here, dst_ref=here,
            send_sem=d2d_send, recv_sem=d2d_recv.at[head],
            device_id={"tp": 1 - tp}, device_id_type=MESH,
        )

    pltpu.make_async_copy(w_buf, w_buf, w_sem).wait()
    for head in range(mine):

        @pl.when(has_prev2)
        def _():
            settle(stat_in.at[head], stat_recv.at[head])
            settle(part_in.at[head], part_recv.at[head])

        @pl.when(has_prev)
        def _():
            settle(mark_in.at[head], mark_recv.at[head])
            settle(near_in.at[head, pl.ds(0, near_out.shape[1])], near_recv.at[head])

        for d in (3, 1, 2, 0):
            j = partner(d)
            if d:
                merge(j, head, att.at[head, j], att_stat.at[head, j])
                for copy in home(d, head):
                    copy.start()
            else:
                merge(j, head, back.at[head, j], back_stat.at[head, j])

    @pl.when(far_next)
    def _():
        edge_hop(K).start()

    @pl.when(relay_next)
    def _():
        settle(relay, relay_recv)
        relay_out().start()

    @pl.when(edge_prev)
    def _():
        settle(kv0.at[:, pl.ds(0, KEYS)], edge_recv)

    group1(0)
    for head in range(mine):
        finish(0, head)
        twin(0, tp, head).start()
    for head in range(mine):
        for d in (1, 2, 3):
            wait_home(d, head)
            finish(d, head)
            twin(d, tp, head).start()
        product = jnp.dot(full[tp, head], w_buf[tp, head], preferred_element_type=F32)
        settle(full.at[1 - tp, head], d2d_recv.at[head])
        product = product + jnp.dot(
            full[1 - tp, head], w_buf[1 - tp, head], preferred_element_type=F32
        )
        if head == 0:
            total_buf[...] = product
        elif head < mine - 1:
            total_buf[...] += product
        else:
            o_ref[...] = (total_buf[...] + product).astype(BF16)

    settle(raw.at[:, :, pl.ds(0, tokens * 2 * (TEAM - 1) // (3 * TEAM))], deal_send)
    settle(back.at[:, pl.ds(0, TEAM - 1)], ret_send.at[0])
    settle(back_stat.at[:, pl.ds(0, TEAM - 1)], ret_send.at[1])
    settle(full.at[tp], d2d_send)

    @pl.when(has_next)
    def _():
        settle(kv2.at[:, :, pl.ds(TEAM, TEAM)], first_send)
        settle(near_out, near_send.at[0])
        settle(mark_out, near_send.at[1])

    @pl.when(edge_next)
    def _():
        settle(kv0.at[:, pl.ds(0, KEYS)], edge_send)

    @pl.when(relay_next)
    def _():
        settle(relay, relay_send)

    @pl.when(has_prev2)
    def _():
        settle(q_next, turn_send)

    @pl.when(has_prev)
    def _():
        settle(q_near, low_send)

    @pl.when(middle)
    def _():
        settle(part_out, part_send.at[0])
        settle(stat_out, part_send.at[1])


def angle_tables(tokens, n_sp):
    inverse = ROPE_BASE ** (-np.arange(0, HEAD, 2) / HEAD)

    def pair(positions):
        angles = positions[:, None] * inverse[None, :]
        cosine, sine = np.cos(angles), np.sin(angles)
        return (
            np.concatenate([cosine, cosine], axis=1),
            np.concatenate([-sine, sine], axis=1),
        )

    by_group = []
    for stride in STRIDES:
        order = np.arange(tokens).reshape(tokens // stride, stride).T.reshape(-1)
        by_group.append(pair(order.astype(np.float64)))
    rows = np.stack([np.stack([t[i] for t in by_group]) for i in range(2)])
    base = np.zeros((n_sp, 8, HEAD))
    base[:, 0], base[:, 1] = pair(np.arange(n_sp) * float(tokens))
    return np.concatenate([rows.reshape(-1, HEAD), base.reshape(-1, HEAD)]).astype(np.float32)


def shards(n_sp, queries, keys, values, w_out):
    tokens, width = queries.shape[1:]
    heads = width // HEAD
    mine = heads // TEAM
    part = mine * HEAD
    span = TEAM * tokens
    low = KEYS * STRIDES[1] // tokens
    angles = angle_tables(tokens, n_sp)
    any_spec = pl.BlockSpec(memory_space=pl.ANY)
    vmem = pl.BlockSpec(memory_space=pltpu.VMEM)
    dma = pltpu.SemaphoreType.DMA
    return pl.pallas_call(
        functools.partial(kernel, (tokens, n_sp, heads)),
        out_shape=jax.ShapeDtypeStruct((tokens, w_out.shape[1]), BF16),
        in_specs=[any_spec] * 5,
        out_specs=vmem,
        scratch_shapes=[
            pltpu.VMEM((3, 3, tokens, width), BF16),
            pltpu.VMEM((3, 2, TEAM, mine, tokens, HEAD), BF16),
            pltpu.VMEM((tokens, width), BF16),
            pltpu.VMEM((2, mine, TEAM * HEAD, w_out.shape[1]), BF16),
            pltpu.VMEM(angles.shape, F32),
            pltpu.VMEM((2, 3, tokens, HEAD), F32),
            pltpu.VMEM((2, tokens, tokens), BF16),
            pltpu.VMEM((2, mine, TEAM, tokens, HEAD), BF16),
            pltpu.VMEM((mine, TEAM, tokens, HEAD), BF16),
            pltpu.VMEM((mine, low, tokens, HEAD), BF16),
            pltpu.VMEM((2, KEYS + tokens, width), BF16),
            pltpu.VMEM((2, mine, TEAM, tokens, HEAD), BF16),
            pltpu.VMEM((2, mine, 2 * TEAM, tokens, HEAD), BF16),
            pltpu.VMEM((KEYS, width), BF16),
            pltpu.VMEM((4, mine, span, HEAD), F32),
            pltpu.VMEM((4, mine, span, HEAD), F32),
            pltpu.VMEM((heads, tokens, HEAD), F32),
            pltpu.VMEM((heads, tokens, HEAD), F32),
            pltpu.VMEM((3, KEYS, 2 * KEYS), F32),
            pltpu.VMEM((mine, span, HEAD), BF16),
            pltpu.VMEM((mine, span // KEYS, KEYS), F32),
            pltpu.VMEM((mine, span, HEAD), BF16),
            pltpu.VMEM((mine, span // KEYS, KEYS), F32),
            pltpu.VMEM((mine, low * tokens, HEAD), BF16),
            pltpu.VMEM((mine, span // KEYS, KEYS), F32),
            pltpu.VMEM((mine, span, HEAD), BF16),
            pltpu.VMEM((mine, span // KEYS, KEYS), F32),
            pltpu.VMEM((mine, TEAM, tokens, HEAD), BF16),
            pltpu.VMEM((mine, TEAM, 8, KEYS), F32),
            pltpu.VMEM((mine, TEAM, tokens, HEAD), BF16),
            pltpu.VMEM((mine, TEAM, 8, KEYS), F32),
            pltpu.VMEM((2, mine, tokens, TEAM * HEAD), BF16),
            pltpu.VMEM((tokens, w_out.shape[1]), F32),
            dma((3, 3)),
            dma,
            dma,
            dma,
            dma((4, mine, TEAM - 1)),
            dma((mine,)),
            dma,
            dma((mine,)),
            dma,
            dma((mine,)),
            dma,
            dma((mine,)),
            dma,
            dma,
            dma,
            dma,
            dma((2,)),
            dma((mine,)),
            dma((mine,)),
            dma((2,)),
            dma((mine,)),
            dma((mine,)),
            dma((2,)),
            dma((TEAM - 1, mine)),
            dma((TEAM - 1, mine)),
            dma,
            dma((mine,)),
        ],
        compiler_params=pltpu.CompilerParams(
            collective_id=0, has_side_effects=True, vmem_limit_bytes=53 * 1024 * 1024
        ),
    )(queries, keys, values, w_out, jnp.asarray(angles))


def solution(mesh):
    return jax.shard_map(
        functools.partial(shards, mesh.shape["sp"]),
        mesh=mesh,
        in_specs=(P(None, "sp", "tp"), P(None, "sp", "tp"), P(None, "sp", "tp"), P(None, "tp")),
        out_specs=P("sp", "tp"),
        check_vma=False,
    )
```

time: 70.7 us -> 59.9 us (0.85)
  Pallas kernels: 69.3 us -> 58.5 us
    pallas_call x1, Pallas kernels: 69.3 us -> 58.5 us  [shards(): pl.pallas_call(functools.partial(kernel, (tokens, n_sp, heads)), out_shap...]
where the time goes in v3:
time: 59.9 us; the launch traced here: 59.3 us
  Pallas kernels  58.5 us (98%)
  local copies, waits for them, and re-layouts  0.8 us (1%)
    pallas_call x1, Pallas kernels, shards(): pl.pallas_call(functools.partial(kernel, (tokens, n_sp, heads)), out_shap...  58.5 us

profile of v3, /device:TPU:17, one launch (start us, length us, event | category | flops | bytes accessed | tf_op | source)
XLA Modules:
  0.0 59.3 jit_solution(14464394662029017238)
XLA Ops:
  0.0 58.5 %shard_map.55 = bf16[256,1024]{1,0:T(8,128)(2,1)S(1)} custom-call(bf16[3,256,1024]{2,1,0:T(8,128)(2,1)} %q_in.1, bf16[3,256,1024]{2,1,0:T(8,128)(2,1)} %k_in.1, bf16[3,256,1024]{2,1,0:T(8,128)(2,1)} %v_in.1, bf16[2048,1024]{1,0:T(8,128)(2,1)} %w_in.1, f32[1664,128]{1,0:T(8,128)} %constant.2.clone.angles_in), custom_call_target="tpu_custom_call" | custom-call | tf_op jit(solution)/shard_map/pallas_call | solution.py:692
  58.5 0.8 %copy.7 = bf16[256,1024]{1,0:T(8,128)(2,1)} copy(bf16[256,1024]{1,0:T(8,128)(2,1)S(1)} %shard_map.55) | data formatting | bytes 1048576

commit v4 on v3

--- a/solution.py
+++ b/solution.py
@@ -607,22 +607,23 @@
     for head in range(mine):
         finish(0, head)
         twin(0, tp, head).start()
+    def mixed(half, head):
+        return jnp.dot(full[half, head], w_buf[half, head], preferred_element_type=F32)
+
     for head in range(mine):
-        for d in (1, 2, 3):
+        for d in (3, 2, 1):
             wait_home(d, head)
             finish(d, head)
             twin(d, tp, head).start()
-        product = jnp.dot(full[tp, head], w_buf[tp, head], preferred_element_type=F32)
+        if head:
+            total_buf[...] += mixed(tp, head)
+        else:
+            total_buf[...] = mixed(tp, head)
         settle(full.at[1 - tp, head], d2d_recv.at[head])
-        product = product + jnp.dot(
-            full[1 - tp, head], w_buf[1 - tp, head], preferred_element_type=F32
-        )
-        if head == 0:
-            total_buf[...] = product
-        elif head < mine - 1:
-            total_buf[...] += product
+        if head < mine - 1:
+            total_buf[...] += mixed(1 - tp, head)
         else:
-            o_ref[...] = (total_buf[...] + product).astype(BF16)
+            o_ref[...] = (total_buf[...] + mixed(1 - tp, head)).astype(BF16)
 
     settle(raw.at[:, :, pl.ds(0, tokens * 2 * (TEAM - 1) // (3 * TEAM))], deal_send)
     settle(back.at[:, pl.ds(0, TEAM - 1)], ret_send.at[0])

time: 59.9 us -> 59.2 us (0.988)
  no operation moved by 1% of the time
where the time goes in v4:
time: 59.2 us; the launch traced here: 59.1 us
  Pallas kernels  58.3 us (98%)
  local copies, waits for them, and re-layouts  0.8 us (1%)
    pallas_call x1, Pallas kernels, shards(): pl.pallas_call(functools.partial(kernel, (tokens, n_sp, heads)), out_shap...  58.3 us

profile of v4, /device:TPU:17, one launch (start us, length us, event | category | flops | bytes accessed | tf_op | source)
XLA Modules:
  0.0 59.1 jit_solution(11202974788888861941)
XLA Ops:
  0.0 58.3 %shard_map.55 = bf16[256,1024]{1,0:T(8,128)(2,1)S(1)} custom-call(bf16[3,256,1024]{2,1,0:T(8,128)(2,1)} %q_in.1, bf16[3,256,1024]{2,1,0:T(8,128)(2,1)} %k_in.1, bf16[3,256,1024]{2,1,0:T(8,128)(2,1)} %v_in.1, bf16[2048,1024]{1,0:T(8,128)(2,1)} %w_in.1, f32[1664,128]{1,0:T(8,128)} %constant.2.clone.angles_in), custom_call_target="tpu_custom_call" | custom-call | tf_op jit(solution)/shard_map/pallas_call | solution.py:693
  58.3 0.8 %copy.7 = bf16[256,1024]{1,0:T(8,128)(2,1)} copy(bf16[256,1024]{1,0:T(8,128)(2,1)S(1)} %shard_map.55) | data formatting | bytes 1048576

commit v5 on v4

--- a/solution.py
+++ b/solution.py
@@ -14,6 +14,7 @@
 ROPE_BASE = 10000.0
 MASKED = -1e30
 TEAM = 4
+TAGS = 16
 
 MESH = pl.DeviceIdType.MESH
 F32 = jnp.float32
@@ -28,11 +29,11 @@
     raw, ready, q_home, w_buf, angles, tables, perms,
     q_buf, q_next, q_near, kv0, kv1, kv2, relay, acc, lse, acc1, lse1, bias,
     part_out, stat_out, part_in, stat_in, near_out, mark_out, near_in, mark_in,
-    att, att_stat, back, back_stat, full, total_buf,
-    in_sem, w_sem, angles_sem, deal_send, deal_recv, pair_recv, first_send, first_recv,
+    att, back, full, total_buf,
+    in_sem, w_sem, angles_sem, deal_send, deal_recv, low_deal, pair_recv, first_send, first_recv,
     turn_send, turn_recv, low_send, low_recv, edge_send, edge_recv, relay_send, relay_recv,
     part_send, part_recv, stat_recv, near_send, near_recv, mark_recv,
-    ret_send, ret_recv, tag_recv, d2d_send, d2d_recv,
+    ret_send, ret_recv, d2d_send, d2d_recv,
 ):
     tokens, n_sp, heads = cfg
     width = heads * HEAD
@@ -149,7 +150,9 @@
     def recv_of(kind, g, head, d):
         if g == 1 and kind != Q:
             return pair_recv.at[head]
-        return deal_recv.at[kind if g == 2 else 3, head, d - 1]
+        if g == 1:
+            return low_deal.at[head]
+        return deal_recv.at[kind, head, d - 1]
 
     def deal(kind, g, head, d):
         return pltpu.make_async_remote_copy(
@@ -232,9 +235,12 @@
             pl.when(has_prev & (s < low))(lambda: low_hop(head, s).start())
 
     def arrive(kind, g, head):
+        if g == 1:
+            settle(q_buf.at[0, head, pl.ds(0, TEAM - 1)], low_deal.at[head])
         for d in (1, 2, 3):
             s = partner(d)
-            settle(slot(kind, g, head, s), recv_of(kind, g, head, d))
+            if g == 2:
+                settle(slot(kind, g, head, s), recv_of(kind, g, head, d))
             forward(kind, g, head, s)
 
     def send_first(kind, g, first=False):
@@ -303,7 +309,7 @@
 
     @pl.when(edge_next & (me < TEAM - 1))
     def _():
-        for kind in (V, K):
+        for kind in (K, V):
             edge_hop(kind).start()
 
     @pl.when(far_next)
@@ -474,7 +480,7 @@
                 part_hop(head, j).start()
             stat_hop(head).start()
 
-    def here(head):
+    def local(head):
         group3(head, q_buf.at[1, head], 2 * TEAM, bias[2, 0:lot, 0 : 2 * lot], 1)
 
     def low_pass(head):
@@ -496,20 +502,23 @@
     pass_on(0)
     arrive(K, 2, 1)
     pass_send(0)
-    here(0)
+    local(0)
     arrive(Q, 2, 1)
     first_done(1)
     arrive(Q, 1, 0)
     pass_on(1)
     pass_send(1)
-    here(1)
+    local(1)
     low_pass(0)
     arrive(Q, 1, 1)
     low_pass(1)
 
     group2()
 
-    def merge(j, head, out_ref, log_ref):
+    tag_row = lax.broadcasted_iota(jnp.int32, (TAGS, KEYS), 0)
+
+    def merge(j, head, out_ref):
+        tags = jnp.zeros((TAGS, KEYS), F32)
         for c in range(chunks):
             rows = pl.ds(pl.multiple_of(j * tokens + c * KEYS, KEYS), KEYS)
             logs = [lse[g, head, rows, :] for g in range(2)]
@@ -523,38 +532,35 @@
             lower = sum(scales)
             upper = sum(x * y for x, y in zip(scales, outs))
             out_ref[c * KEYS : (c + 1) * KEYS, :] = (upper / lower).astype(BF16)
-            log_ref[c : c + 1, :] = to_row(peak + jnp.log(lower))
+            rest = to_row(peak + jnp.log(lower))
+            for i in range(3):
+                piece = rest.astype(BF16).astype(F32)
+                tags = jnp.where(tag_row == 3 * c + i, piece, tags)
+                rest = rest - piece
+        out_ref[tokens:, :] = tags.astype(BF16)
 
     def place_of(s):
         return pl.ds(pl.multiple_of(s * HEAD, HEAD), HEAD)
 
     def home(d, head):
         peer = partner(d)
-        where = {"sp": team * TEAM + peer}
-        return (
-            pltpu.make_async_remote_copy(
-                src_ref=att.at[head, peer], dst_ref=back.at[head, me],
-                send_sem=ret_send.at[0], recv_sem=ret_recv.at[d - 1, head],
-                device_id=where, device_id_type=MESH,
-            ),
-            pltpu.make_async_remote_copy(
-                src_ref=att_stat.at[head, peer], dst_ref=back_stat.at[head, me],
-                send_sem=ret_send.at[1], recv_sem=tag_recv.at[d - 1, head],
-                device_id=where, device_id_type=MESH,
-            ),
+        return pltpu.make_async_remote_copy(
+            src_ref=att.at[head, peer], dst_ref=back.at[head, me],
+            send_sem=ret_send, recv_sem=ret_recv.at[d - 1, head],
+            device_id={"sp": team * TEAM + peer}, device_id_type=MESH,
         )
 
     def wait_home(d, head):
         settle(back.at[head, partner(d)], ret_recv.at[d - 1, head])
-        settle(back_stat.at[head, partner(d)], tag_recv.at[d - 1, head])
 
     def finish(d, head):
         s = partner(d)
         h = s * mine + head
+        tags = back[head, s, tokens:, :].astype(F32)
         for c in range(chunks):
             rows = slice(c * KEYS, (c + 1) * KEYS)
             log_a = lse1[h, rows, :]
-            log_b = to_col(back_stat[head, s, c : c + 1, :])
+            log_b = to_col(jnp.sum(jnp.where(tag_row // 3 == c, tags, 0.0), axis=0, keepdims=True))
             peak = jnp.maximum(log_a, log_b)
             scale_a, scale_b = jnp.exp(log_a - peak), jnp.exp(log_b - peak)
             upper = scale_a * acc1[h, rows, :] + scale_b * back[head, s, rows, :].astype(F32)
@@ -581,14 +587,13 @@
             settle(mark_in.at[head], mark_recv.at[head])
             settle(near_in.at[head, pl.ds(0, near_out.shape[1])], near_recv.at[head])
 
-        for d in (3, 1, 2, 0):
+        for d in (1, 3, 2, 0):
             j = partner(d)
             if d:
-                merge(j, head, att.at[head, j], att_stat.at[head, j])
-                for copy in home(d, head):
-                    copy.start()
+                merge(j, head, att.at[head, j])
+                home(d, head).start()
             else:
-                merge(j, head, back.at[head, j], back_stat.at[head, j])
+                merge(j, head, back.at[head, j])
 
     @pl.when(far_next)
     def _():
@@ -611,14 +616,15 @@
         return jnp.dot(full[half, head], w_buf[half, head], preferred_element_type=F32)
 
     for head in range(mine):
-        for d in (3, 2, 1):
+        for d in (1, 2, 3):
             wait_home(d, head)
             finish(d, head)
             twin(d, tp, head).start()
+        if head == 0:
+            total_buf[...] = mixed(tp, head)
+    for head in range(mine):
         if head:
             total_buf[...] += mixed(tp, head)
-        else:
-            total_buf[...] = mixed(tp, head)
         settle(full.at[1 - tp, head], d2d_recv.at[head])
         if head < mine - 1:
             total_buf[...] += mixed(1 - tp, head)
@@ -626,8 +632,7 @@
             o_ref[...] = (total_buf[...] + mixed(1 - tp, head)).astype(BF16)
 
     settle(raw.at[:, :, pl.ds(0, tokens * 2 * (TEAM - 1) // (3 * TEAM))], deal_send)
-    settle(back.at[:, pl.ds(0, TEAM - 1)], ret_send.at[0])
-    settle(back_stat.at[:, pl.ds(0, TEAM - 1)], ret_send.at[1])
+    settle(back.at[:, pl.ds(0, TEAM - 1)], ret_send)
     settle(full.at[tp], d2d_send)
 
     @pl.when(has_next)
@@ -723,17 +728,16 @@
             pltpu.VMEM((mine, span // KEYS, KEYS), F32),
             pltpu.VMEM((mine, span, HEAD), BF16),
             pltpu.VMEM((mine, span // KEYS, KEYS), F32),
-            pltpu.VMEM((mine, TEAM, tokens, HEAD), BF16),
-            pltpu.VMEM((mine, TEAM, 8, KEYS), F32),
-            pltpu.VMEM((mine, TEAM, tokens, HEAD), BF16),
-            pltpu.VMEM((mine, TEAM, 8, KEYS), F32),
+            pltpu.VMEM((mine, TEAM, tokens + TAGS, HEAD), BF16),
+            pltpu.VMEM((mine, TEAM, tokens + TAGS, HEAD), BF16),
             pltpu.VMEM((2, mine, tokens, TEAM * HEAD), BF16),
             pltpu.VMEM((tokens, w_out.shape[1]), F32),
             dma((3, 3)),
             dma,
             dma,
             dma,
-            dma((4, mine, TEAM - 1)),
+            dma((3, mine, TEAM - 1)),
+            dma((mine,)),
             dma((mine,)),
             dma,
             dma((mine,)),
@@ -751,8 +755,7 @@
             dma((2,)),
             dma((mine,)),
             dma((mine,)),
-            dma((2,)),
-            dma((TEAM - 1, mine)),
+            dma,
             dma((TEAM - 1, mine)),
             dma,
             dma((mine,)),

time: 59.2 us -> 59 us (level)
  no operation moved by 1% of the time
where the time goes in v5:
time: 59 us; the launch traced here: 58.9 us
  Pallas kernels  58.1 us (98%)
  local copies, waits for them, and re-layouts  0.8 us (1%)
    pallas_call x1, Pallas kernels, shards(): pl.pallas_call(functools.partial(kernel, (tokens, n_sp, heads)), out_shap...  58.1 us

profile of v5, /device:TPU:17, one launch (start us, length us, event | category | flops | bytes accessed | tf_op | source)
XLA Modules:
  0.0 58.9 jit_solution(7600981332063674111)
XLA Ops:
  0.0 58.1 %shard_map.55 = bf16[256,1024]{1,0:T(8,128)(2,1)S(1)} custom-call(bf16[3,256,1024]{2,1,0:T(8,128)(2,1)} %q_in.1, bf16[3,256,1024]{2,1,0:T(8,128)(2,1)} %k_in.1, bf16[3,256,1024]{2,1,0:T(8,128)(2,1)} %v_in.1, bf16[2048,1024]{1,0:T(8,128)(2,1)} %w_in.1, f32[1664,128]{1,0:T(8,128)} %constant.2.clone.angles_in), custom_call_target="tpu_custom_call" | custom-call | tf_op jit(solution)/shard_map/pallas_call | solution.py:698
  58.1 0.8 %copy.7 = bf16[256,1024]{1,0:T(8,128)(2,1)} copy(bf16[256,1024]{1,0:T(8,128)(2,1)S(1)} %shard_map.55) | data formatting | bytes 1048576
